TPU v7x, 512 devices: a whole 4x4x16 slice. The times are simulated.
512 devices in a mesh: sp: 64 (over z, y), tp: 8 (over x, core).
Axes of the slice: x: 4, y: 4, z: 16, core: 2. Of those that a mesh axis runs over, the one named last changes fastest.
Arguments:
- tokens: bfloat16 [16384, 2048], P('sp'), may hold values from -6 to 6
- input_norm_gain: float32 [2048], replicated, may hold values from 0.1 to 1.9
- mq_weight: bfloat16 [2048, 1024], P('sp', 'tp'), may hold values from -0.125 to 0.125
- mk_weight: bfloat16 [2048, 1024], P('sp', 'tp'), may hold values from -0.125 to 0.125
- mv_weight: bfloat16 [2048, 1024], P('sp', 'tp'), may hold values from -0.125 to 0.125
- mo_weight: bfloat16 [2048, 1024], P('sp', 'tp'), may hold values from -0.125 to 0.125
- gate_weight: bfloat16 [2048, 4, 8], P('sp', None, 'tp'), may hold values from -0.125 to 0.125
- gate_bias: float32 [4, 8], P(None, 'tp'), may hold values from -3 to 100
- decay_extra: float32 [2, 8, 16384], P(None, 'tp', 'sp'), may hold values from -1 to 0
- m_gain: float32 [1024], P('tp'), may hold values from 0.1 to 1.9
- aq_weight: bfloat16 [2048, 1024], P('sp', 'tp'), may hold values from -0.125 to 0.125
- ak_weight: bfloat16 [2048, 512], P('sp', 'tp'), may hold values from -8.838835 to 8.838835
- av_weight: bfloat16 [2048, 512], P('sp', 'tp'), may hold values from -0.125 to 0.125
- sink_logit: float32 [16], P('tp'), may hold values from 3 to 6
- out_m_weight: bfloat16 [1024, 2048], P('sp', 'tp'), may hold values from -0.1875 to 0.1875
- out_a_weight: bfloat16 [1024, 2048], P('sp', 'tp'), may hold values from -1.5 to 1.5
Outputs:
- mixed: bfloat16 [16384, 2048], P('sp', 'tp')
- log_total: float32 [16, 16384], P('tp', 'sp')
All inputs are finite; a program needn't handle non-finite values.
Results may differ from a plain program's by a relative error of at most 0.015.
The roundings to bfloat16 on the way count: a program that leaves them out, or rounds other values in their place, can miss the bound.
Values may be sent and summed in bfloat16 or wider, within the bound.
A program may use at most 64 MiB of HBM per device.

v0:
```python
import jax
import jax.numpy as jnp
from jax import lax
from jax.sharding import Mesh
from jax.sharding import PartitionSpec as P

M_DIM = 128
W_DIM = 64
WINDOW = 128
M_BLOCK = 64
SP = ("sp_0", "sp_1")


EPS = 1e-06
FLOOR_LOG = -1e30


def sent_together(arrays, axis, dim, along):
    ends, at = ([], 0)
    for a in arrays[:-1]:
        at += a.shape[along]
        ends.append(at)
    both = jnp.concatenate(arrays, axis=along)
    return tuple(jnp.split(lax.all_gather(both, axis, axis=dim, tiled=True), ends, axis=along))


def sent_together_2(arrays, axis, dim, along):
    columns = [a.reshape(*a.shape[:along], -1) for a in arrays]
    both = jnp.concatenate(columns, axis=along)
    out, at, outs = (lax.all_gather(both, axis, axis=dim, tiled=True), 0, [])
    for a, column in zip(arrays, columns):
        share = out[..., at : at + column.shape[along]]
        outs.append(share.reshape(*share.shape[:along], *a.shape[along:]))
        at += column.shape[along]
    return tuple(outs)


def with_halo(x, sides, width):
    for axis, dim in sides:
        peers, length = (lax.axis_size(axis), x.shape[dim])
        up = [(i, (i + 1) % peers) for i in range(peers - 1)]
        down = [(j, i) for i, j in up]
        last = lax.slice_in_dim(x, length - width, length, axis=dim)
        first = lax.slice_in_dim(x, 0, width, axis=dim)
        before = lax.ppermute(last, axis, up)
        after = lax.ppermute(first, axis, down)
        x = jnp.concatenate([before, x, after], axis=dim)
    return x


def gathered_by_axis(x, axes, dim):
    for axis in reversed(axes):
        x = lax.all_gather(x, axis, axis=dim, tiled=True)
    return x


def rms_rows(inputs, gain_vec):
    return inputs * lax.rsqrt(jnp.mean(inputs * inputs, axis=-1, keepdims=True) + EPS) * gain_vec


def stored(result):
    return lax.optimization_barrier(result.astype(jnp.bfloat16))


def flip_tokens(array_in):
    return jnp.flip(array_in, axis=1)


def block_pass(queries, key_vecs, value_vecs, in_gate, log_forget, start_state):
    head_count, length, head_width = queries.shape
    block_count = length // M_BLOCK

    def blocks(array_in):
        return jnp.moveaxis(
            array_in.reshape((head_count, block_count, M_BLOCK) + array_in.shape[2:]), 1, 0
        )

    lower_mask = jnp.tril(jnp.ones((M_BLOCK, M_BLOCK), dtype=bool))

    def advance(state_in, block_in):
        cell_mat, norm_vec, stab_max = state_in
        q_blk, k_blk, v_blk, i_blk, f_blk = block_in
        cum_log = jnp.cumsum(f_blk, axis=-1)
        seg_total = cum_log[:, -1]
        log_end = seg_total[:, None] - cum_log + i_blk
        max_next = jnp.maximum(seg_total + stab_max, jnp.max(log_end, axis=-1))
        w_end = jnp.exp(log_end - max_next[:, None])
        fade_old = jnp.exp(seg_total + stab_max - max_next)
        cell_next = fade_old[:, None, None] * cell_mat + jnp.einsum(
            "hsv,hsk->hvk", w_end[:, :, None] * v_blk, k_blk
        )
        norm_next = fade_old[:, None] * norm_vec + jnp.einsum("hs,hsk->hk", w_end, k_blk)
        log_w = jnp.where(
            lower_mask, cum_log[:, :, None] - cum_log[:, None, :] + i_blk[:, None, :], -jnp.inf
        )
        log_inter = cum_log + stab_max[:, None]
        row_max = jnp.maximum(log_inter, jnp.max(log_w, axis=-1))
        w_intra = jnp.exp(log_w - row_max[:, :, None])
        w_inter = jnp.exp(log_inter - row_max)
        scores = jnp.einsum("htk,hsk->hts", q_blk, k_blk) * w_intra
        numerator = jnp.einsum("hts,hsv->htv", scores, v_blk) + w_inter[..., None] * jnp.einsum(
            "hvk,htk->htv", cell_mat, q_blk
        )
        denominator = jnp.sum(scores, axis=-1) + w_inter * jnp.einsum("hk,htk->ht", norm_vec, q_blk)
        result_rows = numerator / jnp.maximum(jnp.abs(denominator), jnp.exp(-row_max))[..., None]
        return ((cell_next, norm_next, max_next), result_rows)

    final_state, outputs = lax.scan(
        advance,
        start_state,
        tuple(
            (blocks(array_in) for array_in in (queries, key_vecs, value_vecs, in_gate, log_forget))
        ),
    )
    return (jnp.moveaxis(outputs, 0, 1).reshape(head_count, length, head_width), final_state)


def summarize(key_vecs, value_vecs, in_gate, log_forget):
    cum_log = jnp.cumsum(log_forget, axis=-1)
    seg_total = cum_log[:, -1]
    log_end = seg_total[:, None] - cum_log + in_gate
    peak_log = jnp.max(log_end, axis=-1)
    weights_end = jnp.exp(log_end - peak_log[:, None])
    cell_mat = jnp.einsum("hsv,hsk->hvk", weights_end[:, :, None] * value_vecs, key_vecs)
    norm_vec = jnp.einsum("hs,hsk->hk", weights_end, key_vecs)
    return (seg_total, cell_mat, norm_vec, peak_log)


def merge_side(state_in, cell_mats, norm_vecs, logs, usable):
    cell_mat, norm_vec, peak_log = state_in
    masked = jnp.where(usable, logs, FLOOR_LOG)
    new_peak = jnp.maximum(peak_log, jnp.max(masked, axis=0))
    scales = jnp.where(usable, jnp.exp(masked - new_peak[None]), 0.0)
    cell_mat = jnp.einsum("jh,jhvk->hvk", scales, cell_mats)
    norm_vec = jnp.einsum("jh,jhk->hk", scales, norm_vecs)
    return (cell_mat, norm_vec, new_peak)


def gather_states(forward_sum, backward_sum):
    decay_all = sent_together((forward_sum[0][None], backward_sum[0][None]), SP, 0, 1)
    own_index = lax.axis_index(SP)
    acc_fwd = jnp.cumsum(decay_all[0], axis=0)
    acc_bwd = jnp.cumsum(decay_all[1], axis=0)
    before_own = lax.dynamic_index_in_dim(acc_fwd - decay_all[0], own_index, 0, keepdims=False)
    after_own = lax.dynamic_index_in_dim(acc_bwd, own_index, 0, keepdims=False)
    lead_bwd = acc_bwd - decay_all[1]
    empty_side = (
        jnp.zeros_like(forward_sum[1]),
        jnp.zeros_like(forward_sum[2]),
        jnp.full_like(forward_sum[3], FLOOR_LOG),
    )
    state_in = empty_side + empty_side
    pieces = sent_together_2(
        (
            forward_sum[1][None],
            forward_sum[2][None],
            forward_sum[3][None],
            backward_sum[1][None],
            backward_sum[2][None],
            backward_sum[3][None],
        ),
        SP,
        0,
        2,
    )
    piece_count = pieces[0].shape[0]
    device_ids = jnp.arange(piece_count, dtype=jnp.int32)
    log_fwd = before_own[None] - acc_fwd + pieces[2]
    log_bwd = lead_bwd - after_own[None] + pieces[5]
    left_side = merge_side(
        state_in[:3], pieces[0], pieces[1], log_fwd, (device_ids < own_index)[:, None]
    )
    right_side = merge_side(
        state_in[3:], pieces[3], pieces[4], log_bwd, (device_ids > own_index)[:, None]
    )
    states = left_side + right_side
    return (states[:3], states[3:])


def window_attend(a_query, kv_pairs, sink_logit, first_row, total_rows):
    tok_rows = a_query.shape[0]
    block_len = WINDOW
    block_count = tok_rows // block_len
    kv_width = kv_pairs.shape[1] // 2
    kv_heads = kv_width // W_DIM
    q_heads = a_query.shape[1] // W_DIM
    groups = q_heads // kv_heads
    filled_margin = with_halo(kv_pairs, ((SP, 0),), WINDOW)
    windows = jnp.concatenate(
        [
            filled_margin[place_idx * block_len : place_idx * block_len + tok_rows].reshape(
                block_count, block_len, 2 * kv_width
            )
            for place_idx in range(3)
        ],
        axis=1,
    )
    key_block = windows[:, :, :kv_width].reshape(block_count, 3 * block_len, kv_heads, W_DIM)
    content_tile = windows[:, :, kv_width:].reshape(block_count, 3 * block_len, kv_heads, W_DIM)
    query_block = a_query.reshape(block_count, block_len, kv_heads, groups, W_DIM)
    scores = jnp.einsum(
        "nqgrd,nkgd->ngrqk", query_block, key_block, preferred_element_type=jnp.float32
    ) * W_DIM ** (-0.5)
    query_off = jnp.arange(block_len, dtype=jnp.int32)
    key_off = jnp.arange(3 * block_len, dtype=jnp.int32) - block_len
    in_window = jnp.abs(query_off[:, None] - key_off[None, :]) <= WINDOW
    key_place = (
        first_row + jnp.arange(block_count, dtype=jnp.int32)[:, None] * block_len + key_off[None, :]
    )
    inside = (key_place >= 0) & (key_place < total_rows)
    usable = in_window[None] & inside[:, None, :]
    scores = jnp.where(usable[:, None, None], scores, -jnp.inf)
    sink_col = sink_logit.reshape(kv_heads, groups)[None, :, :, None]
    peak_log = jnp.maximum(sink_col, jnp.max(scores, axis=-1))
    weights_exp = jnp.exp(scores - peak_log[..., None])
    weight_total_sum = jnp.exp(sink_col - peak_log) + jnp.sum(weights_exp, axis=-1)
    weighted = jnp.einsum(
        "ngrqk,nkgd->nqgrd",
        weights_exp.astype(jnp.bfloat16),
        content_tile,
        preferred_element_type=jnp.float32,
    )
    scale_back = jnp.transpose(weight_total_sum, (0, 3, 1, 2))[..., None]
    mixed_rows = (weighted / scale_back).astype(jnp.bfloat16).reshape(tok_rows, q_heads * W_DIM)
    log_total = jnp.transpose(peak_log + jnp.log(weight_total_sum), (1, 2, 0, 3)).reshape(
        q_heads, tok_rows
    )
    return (mixed_rows, log_total)


def on_device(
    tokens,
    input_norm_gain,
    mq_weight,
    mk_weight,
    mv_weight,
    mo_weight,
    gate_weight,
    gate_bias,
    decay_extra,
    m_gain,
    aq_weight,
    ak_weight,
    av_weight,
    sink_logit,
    out_m_weight,
    out_a_weight,
):
    tok_rows = tokens.shape[0]
    normed = rms_rows(tokens.astype(jnp.float32), input_norm_gain).astype(jnp.bfloat16)
    local_heads = gate_weight.shape[2]
    gate_cols = 4 * local_heads
    pieces = sent_together_2(
        (mq_weight, mk_weight, mv_weight, mo_weight, gate_weight, aq_weight, ak_weight, av_weight),
        SP,
        0,
        1,
    )
    piece_rows = pieces[0].shape[0]
    flat_gate = pieces[4].reshape(piece_rows, gate_cols)
    segments = (
        pieces[0],
        pieces[1],
        pieces[2],
        pieces[3],
        flat_gate,
        pieces[5],
        pieces[6],
        pieces[7],
    )
    projected = tuple(
        (jnp.dot(normed, segment, preferred_element_type=jnp.float32) for segment in segments)
    )
    m_query = stored(projected[0])
    m_key = stored(projected[1])
    m_value = stored(projected[2])
    m_out = stored(projected[3])
    gates = projected[4].reshape(tok_rows, 4, local_heads) + gate_bias[None]

    def heads_first(matrix):
        return jnp.transpose(
            matrix.astype(jnp.float32).reshape(tok_rows, local_heads, M_DIM), (1, 0, 2)
        )

    queries = heads_first(m_query)
    key_vecs = heads_first(m_key) * M_DIM ** (-0.5)
    value_vecs = heads_first(m_value)
    in_fwd = gates[:, 0, :].T
    forget_fwd = jax.nn.log_sigmoid(gates[:, 1, :].T) + decay_extra[0]
    in_bwd = flip_tokens(gates[:, 2, :].T)
    forget_bwd = flip_tokens(jax.nn.log_sigmoid(gates[:, 3, :].T) + decay_extra[1])
    queries_bwd = flip_tokens(queries)
    keys_bwd = flip_tokens(key_vecs)
    values_bwd = flip_tokens(value_vecs)
    forward_sum = summarize(key_vecs, value_vecs, in_fwd, forget_fwd)
    backward_sum = summarize(keys_bwd, values_bwd, in_bwd, forget_bwd)
    state_fwd, state_bwd = gather_states(forward_sum, backward_sum)
    hidden_fwd, forward_unused = block_pass(
        queries, key_vecs, value_vecs, in_fwd, forget_fwd, state_fwd
    )
    hidden_bwd, unused_bwd = block_pass(
        queries_bwd, keys_bwd, values_bwd, in_bwd, forget_bwd, state_bwd
    )
    cell_out = hidden_fwd + flip_tokens(hidden_bwd)
    gate_open = jax.nn.sigmoid(m_out.astype(jnp.float32)).reshape(tok_rows, local_heads, M_DIM)
    cell_rows = jnp.transpose(cell_out, (1, 0, 2)) * gate_open
    mixed_m = (
        rms_rows(cell_rows, m_gain.reshape(local_heads, M_DIM))
        .astype(jnp.bfloat16)
        .reshape(tok_rows, local_heads * M_DIM)
    )
    a_query = stored(projected[5])
    kv_pairs = jnp.concatenate([stored(projected[6]), stored(projected[7])], axis=1)
    first_row = lax.axis_index(SP) * tok_rows
    total_rows = tok_rows * lax.axis_size(SP)
    mixed_a, log_total = window_attend(a_query, kv_pairs, sink_logit, first_row, total_rows)
    full_m, full_a = sent_together((mixed_m, mixed_a), "tp", 1, 0)
    pieces = (gathered_by_axis(out_m_weight, SP, 0), gathered_by_axis(out_a_weight, SP, 0))
    running = jnp.dot(full_m, pieces[0], preferred_element_type=jnp.float32)
    mixed = running + jnp.dot(full_a, pieces[1], preferred_element_type=jnp.float32)
    return (mixed.astype(jnp.bfloat16), log_total)


def solution(mesh):
    split = Mesh(mesh.devices.reshape(16, 4, mesh.shape["tp"]), ("sp_0", "sp_1", "tp"))
    return jax.shard_map(
        on_device,
        mesh=split,
        in_specs=(
            P(SP, None),
            P(),
            P(SP, "tp"),
            P(SP, "tp"),
            P(SP, "tp"),
            P(SP, "tp"),
            P(SP, None, "tp"),
            P(None, "tp"),
            P(None, "tp", SP),
            P("tp"),
            P(SP, "tp"),
            P(SP, "tp"),
            P(SP, "tp"),
            P("tp"),
            P(SP, "tp"),
            P(SP, "tp"),
        ),
        out_specs=(P(SP, "tp"), P("tp", SP)),
        check_vma=False,
    )
```

profile of v0, /device:TPU:6, one launch (start us, length us, event | category | flops | bytes accessed | tf_op | source)
XLA Modules:
  0.0 497.7 jit_solution(1087127401217503455)
XLA Ops:
  7.2 0.8 copy.130
  8.1 1.5 concatenate.25
  9.7 1.5 fusion.100
  11.9 149.1 %all-gather.5.cloned.1.call-done = bf16[2048,772]{1,0:T(8,128)(2,1)} async-done(((bf16[32,772]{1,0:T(8,128)(2,1)}), bf16[2048,772]{1,0:T(8,128)(2,1)}) %all-gather.5.cloned.1.call-update) | async-done | bytes 3162128 | tf_op jit(solution)/shard_map/all_gather | solution.py:30
  161.0 1.8 fusion.106
  164.3 1.2 fusion.144
  167.8 1.9 fusion.183
  169.8 1.3 subtract_exponential_fusion.5
  171.1 1.5 convolution_convert_fusion.3
  172.7 1.5 convolution_convert_fusion.4
  174.4 1.4 fusion.152
  176.5 1.4 fusion.107
  178.6 1.3 dynamic-update-slice.6
  180.2 0.8 dynamic-update-slice.8
  182.3 1.4 maximum_bitcast_fusion
  183.7 72.1 %all-gather = f32[64,1,2]{2,1,0:T(1,128)S(1)} all-gather(f32[1,1,2]{2,1,0:T(1,128)S(1)} %maximum_bitcast_fusion), channel_id=1, replica_groups=mesh['sp_0'=16,'sp_1'=4,'tp'=8] {'sp_0','sp_1'}, dimensions={0}, use_global_device_ids=true | all-gather | bytes 520 | tf_op jit(solution)/shard_map/all_gather | solution.py:24
  256.6 1.9 convolution_convert_fusion.5
  258.5 1.7 convolution_convert_fusion.6
  260.2 1.3 collective-permute-start.1
  261.5 4.7 collective-permute-start
  266.3 1.2 fusion.197
  267.5 1.8 convolution_convert_fusion
  269.3 1.5 convolution_convert_fusion.1
  270.9 1.6 convolution_convert_fusion.2
  276.9 56.5 %all-gather.7.cloned.1.call-done = f32[64,1,33026]{2,1,0:T(1,128)} async-done(((f32[1,1,33026]{2,1,0:T(1,128)}), f32[64,1,33026]{2,1,0:T(1,128)}) %all-gather.7.cloned.1.call-update) | async-done | bytes 8454672 | tf_op jit(solution)/shard_map/all_gather | solution.py:30
  333.5 0.9 fusion.193
  334.4 1.3 fusion.189
  336.5 11.3 %fusion.194 = (f32[64,1,16384]{2,1,0:T(1,128)S(1)}, f32[64,1,16384]{2,1,0:T(1,128)}) fusion(f32[64,1,33026]{2,1,0:T(1,128)} %all-gather.7.cloned.1.call-done), kind=kLoop, calls=%fused_computation.283 | loop fusion | bytes 16777216 | tf_op jit(solution)/shard_map/slice | solution.py:32
  347.8 2.3 fusion.96
  350.1 1.0 fusion.192
  352.6 4.5 fusion.98
  357.3 22.5 %while.34 = (s32[]{:T(128)}, f32[1,128,128]{2,1,0:T(8,128)S(1)}, f32[1,128]{1,0:T(1,128)S(1)}, f32[1]{0:T(128)}, f32[4,1,64,128]{3,2,1,0:T(8,128)S(1)}, /*index=...) while((s32[]{:T(128)}, f32[1,128,128]{2,1,0:T(8,128)S(1)}, ...), condition=%wide.region_14.15_spmd.clone, body=%wide.region_9.14_spmd.clone.sunk | while | flops 6448260 | bytes 483833 | solution.py:108
  358.1 1.2 fusion.273
  363.8 1.2 fusion.273
  369.4 1.2 fusion.273
  375.0 1.2 fusion.273
  379.8 23.3 %while.35 = (s32[]{:T(128)}, f32[1,128,128]{2,1,0:T(8,128)S(1)}, f32[1,128]{1,0:T(1,128)S(1)}, f32[1]{0:T(128)}, f32[4,1,64,128]{3,2,1,0:T(8,128)S(1)}, /*index=...) while((s32[]{:T(128)}, f32[1,128,128]{2,1,0:T(8,128)S(1)}, ...), condition=%wide.region_22.23_spmd.clone, body=%wide.region_17.22_spmd.clone.sunk | while | flops 6448260 | bytes 483833 | solution.py:108
  380.7 1.2 fusion.292
  384.2 0.8 convolution_add_fusion.7
  386.5 1.2 fusion.292
  392.3 1.2 fusion.292
  398.2 1.2 fusion.292
  404.2 11.9 %all_gather.28 = bf16[64,256]{1,0:T(8,128)(2,1)S(1)} all-gather(bf16[16,256]{1,0:T(8,128)(2,1)S(1)} %copy-done.2), channel_id=1, replica_groups=mesh['sp_0'=16,'sp_1'=4,'tp'=8] {'sp_1'}, dimensions={0}, use_global_device_ids=true | all-gather | bytes 40960 | tf_op jit(solution)/shard_map/all_gather | solution.py:53
  416.1 11.9 %all_gather.30 = bf16[64,256]{1,0:T(8,128)(2,1)S(1)} all-gather(bf16[16,256]{1,0:T(8,128)(2,1)S(1)} %copy-done.3), channel_id=1, replica_groups=mesh['sp_0'=16,'sp_1'=4,'tp'=8] {'sp_1'}, dimensions={0}, use_global_device_ids=true | all-gather | bytes 40960 | tf_op jit(solution)/shard_map/all_gather | solution.py:53
  428.0 31.1 %all_gather.31 = bf16[1024,256]{1,0:T(8,128)(2,1)S(1)} all-gather(bf16[64,256]{1,0:T(8,128)(2,1)S(1)} %all_gather.30), channel_id=1, replica_groups=mesh['sp_0'=16,'sp_1'=4,'tp'=8] {'sp_0'}, dimensions={0}, use_global_device_ids=true | all-gather | bytes 557056 | tf_op jit(solution)/shard_map/all_gather | solution.py:53
  459.1 28.7 %all_gather.29 = bf16[1024,256]{1,0:T(8,128)(2,1)S(1)} all-gather(bf16[64,256]{1,0:T(8,128)(2,1)S(1)} %all_gather.28), channel_id=1, replica_groups=mesh['sp_0'=16,'sp_1'=4,'tp'=8] {'sp_0'}, dimensions={0}, use_global_device_ids=true | all-gather | bytes 557056 | tf_op jit(solution)/shard_map/all_gather | solution.py:53
  487.8 1.3 fusion.113
  489.2 2.0 fusion.105
  (199 shorter events, 39.8 us)
Async XLA Ops:
  7.2 164.0 %copy-start = (bf16[256,2048]{1,0:T(8,128)(2,1)S(1)}, bf16[256,2048]{1,0:T(8,128)(2,1)}, u32[]{:S(2)}) copy-start(bf16[256,2048]{1,0:T(8,128)(2,1)} %param.20) | copy-start | bytes 3145732
  7.2 157.1 %copy-start.5 = (f32[2,1,256]{2,1,0:T(1,128)S(1)}, f32[2,1,256]{2,1,0:T(1,128)}, u32[]{:S(2)}) copy-start(f32[2,1,256]{2,1,0:T(1,128)} %param.28) | copy-start | bytes 6148
  7.2 163.9 %copy-start.7 = (f32[2048]{0:T(1024)S(1)}, f32[2048]{0:T(1024)}, u32[]{:S(2)}) copy-start(f32[2048]{0:T(1024)} %param.21) | copy-start | bytes 24580
  7.2 153.8 %all-gather.5.cloned.1.call-start = ((), (), s32[]{:S(2)}) async-start(), calls=%async_computation | async-start | bytes 3727360 | tf_op jit(solution)/shard_map/all_gather | solution.py:30
  9.6 323.9 %all-gather.7.cloned.1.call-start = ((), (), s32[]{:S(2)}) async-start(), calls=%async_computation.1 | async-start | bytes 8619520 | tf_op jit(solution)/shard_map/all_gather | solution.py:30
  181.0 0.7 copy-start.1
  181.7 306.1 %all-gather.9.cloned.1.call-start = ((), (), s32[]{:S(2)}) async-start(), calls=%async_computation.2 | async-start | bytes 1179648 | tf_op jit(solution)/shard_map/all_gather | solution.py:24
  260.2 14.8 %collective-permute-start.1 = (bf16[128,128]{0,1:T(8,128)(2,1)S(1)}, bf16[128,128]{0,1:T(8,128)(2,1)S(1)}, u32[]{:S(2)}, u32[]{:S(2)}) collective-permute-start(bf16[128,128]{0,1:T(8,128)(2,1)S(1)} %get-tuple-element.329), channel_id=1, source_target_pairs={{8,0},{16,8},{24,16},{32,24},{40,32},{48,40},{56,48},{64,56},{72,6... | collective-permute-start | bytes 98312 | tf_op jit(solution)/shard_map/ppermute | solution.py:46
  261.5 13.6 %collective-permute-start = (bf16[128,128]{0,1:T(8,128)(2,1)S(1)}, bf16[128,128]{0,1:T(8,128)(2,1)S(1)}, u32[]{:S(2)}, u32[]{:S(2)}) collective-permute-start(bf16[128,128]{0,1:T(8,128)(2,1)S(1)} %get-tuple-element.330), channel_id=1, source_target_pairs={{0,8},{8,16},{16,24},{24,32},{32,40},{40,48},{48,56},{56,64},{64,7... | collective-permute-start | bytes 98312 | tf_op jit(solution)/shard_map/ppermute | solution.py:45
  270.9 4.7 copy-start.4
  379.8 23.6 %copy-start.6 = (f32[128]{0:T(128)S(1)}, f32[128]{0:T(128)}, u32[]{:S(2)}) copy-start(f32[128]{0:T(128)} %param.29) | copy-start | bytes 1540
  379.8 24.4 %copy-start.2 = (bf16[16,256]{1,0:T(8,128)(2,1)S(1)}, bf16[16,256]{1,0:T(8,128)(2,1)}, u32[]{:S(2)}) copy-start(bf16[16,256]{1,0:T(8,128)(2,1)} %param.34) | copy-start | bytes 24580
  379.8 36.3 %copy-start.3 = (bf16[16,256]{1,0:T(8,128)(2,1)S(1)}, bf16[16,256]{1,0:T(8,128)(2,1)}, u32[]{:S(2)}) copy-start(bf16[16,256]{1,0:T(8,128)(2,1)} %param.35) | copy-start | bytes 24580
Sparse Core Ops, SparseCore 0:
  11.5 149.4 all-gather.4
  181.8 151.6 all-gather.6
  404.3 24.0 all-gather.8
where the time goes:
time: 499 us; the launch traced here: 498 us
  waiting for transfers between devices  206 us (41%)
  blocking collectives  156 us (31%)
  matrix products  39.7 us (8%)
  other arithmetic  34.5 us (7%)
  local copies, waits for them, and re-layouts  30 us (6%)
  between operations  15.5 us (3%)
  loops' own time  10.4 us (2%)
  starting transfers between devices  6.14 us (1%)
    all_gather x2, waiting for transfers between devices, sent_together_2(): out, at, outs = (lax.all_gather(both, axis, axis=dim, tiled=True), 0, [])  206 us
    all_gather x4, blocking collectives, gathered_by_axis(): x = lax.all_gather(x, axis, axis=dim, tiled=True)  83.6 us
    all_gather x1, blocking collectives, sent_together(): lax.all_gather(both, axis, axis=dim, tiled=True)  72.1 us
    dot_general x8, matrix products, on_device(): jnp.dot(normed, segment, preferred_element_type=jnp.float32)  13.5 us
    slice x3, local copies, waits for them, and re-layouts, sent_together_2(): share = out[..., at:at + column.shape[along]]  13.2 us
    another operation x2, loops' own time, block_pass(): lax.scan(advance, start_state, tuple((blocks(array_in) for array_in in (q...  10.4 us
  transfers between devices with their start and end apart: 5, of which 2 were waited for; matrix products, arithmetic and copies ran while one was open for 4% of the time, Pallas kernels for 0%

commit v1 on v0

v1 whole, which is shorter than its diff:
```python
import functools

import jax
import jax.numpy as jnp
from jax import lax
from jax.experimental import pallas as pl
from jax.experimental.pallas import tpu as pltpu
from jax.sharding import Mesh
from jax.sharding import PartitionSpec as P

M_DIM = 128
W_DIM = 64
WINDOW = 128
EPS = 1e-06
FLOOR_LOG = -1e30
NZ = 16
NY = 4
NT = 8
TOK = 256
D = 2048
SP = ("z", "y")
MESH = pl.DeviceIdType.MESH
VMEM = pltpu.VMEM
F32 = jnp.float32
BF16 = jnp.bfloat16


def mod(a, n):
    return lax.rem(a + n, n)


def remote(src, dst, ssem, rsem, **where):
    return pltpu.make_async_remote_copy(
        src_ref=src,
        dst_ref=dst,
        send_sem=ssem,
        recv_sem=rsem,
        device_id=where,
        device_id_type=MESH,
    )


def gather_body(a_ref, b_ref, ga, gb, ssem, az, ay, ah, bz, by, bh):
    z = lax.axis_index("z")
    y = lax.axis_index("y")
    zu, zd = mod(z + 1, NZ), mod(z - 1, NZ)
    yu, yd = mod(y + 1, NY), mod(y - 1, NY)
    yo = mod(y + 2, NY)
    me = z * NY + y
    barrier = pltpu.get_barrier_semaphore()
    pl.semaphore_signal(barrier, inc=1, device_id={"z": zu}, device_id_type=MESH)
    pl.semaphore_signal(barrier, inc=1, device_id={"z": zd}, device_id_type=MESH)
    pl.semaphore_signal(barrier, inc=1, device_id={"y": yu}, device_id_type=MESH)
    pl.semaphore_signal(barrier, inc=1, device_id={"y": yd}, device_id_type=MESH)
    pl.semaphore_wait(barrier, 4)

    sa, sb = ssem.at[0], ssem.at[1]

    def a_up(src, slot, s):
        return remote(src, ga.at[slot], sa, az.at[0, s], z=zu)

    def a_down(src, slot, s):
        return remote(src, ga.at[slot], sa, az.at[1, s], z=zd)

    def a_side(src, zz):
        slot = zz * NY + y
        remote(src, ga.at[slot], sa, ay.at[0, zz], y=yu).start()
        remote(src, ga.at[slot], sa, ay.at[1, zz], y=yd).start()

    def b_up(src, slot, s, j):
        return remote(src, gb.at[slot], sb, bz.at[0, s, j], z=zu)

    def b_down(src, slot, s, j):
        return remote(src, gb.at[slot], sb, bz.at[1, s, j], z=zd)

    remote(b_ref, gb.at[me], sb, by.at[0], y=yu).start()
    remote(b_ref, gb.at[me], sb, by.at[1], y=yd).start()
    a_up(a_ref, me, 1).start()
    a_down(a_ref, me, 1).start()
    b_up(b_ref, me, 1, y).start()
    b_down(b_ref, me, 1, y).start()
    a_side(a_ref, z)
    ga[me] = a_ref[...]
    gb[me] = b_ref[...]

    slot_d, slot_u, slot_o = z * NY + yd, z * NY + yu, z * NY + yo
    lo, hi = pl.ds(0, 16), pl.ds(16, 16)
    remote(b_ref, gb.at[slot_d], sb, by.at[0], y=yd).wait_recv()
    remote(gb.at[slot_d, lo], gb.at[slot_d, lo], sb, bh.at[0], y=yu).start()
    b_up(gb.at[slot_d], slot_d, 1, yd).start()
    b_down(gb.at[slot_d], slot_d, 1, yd).start()
    remote(b_ref, gb.at[slot_u], sb, by.at[1], y=yd).wait_recv()
    remote(gb.at[slot_u, hi], gb.at[slot_u, hi], sb, bh.at[1], y=yd).start()
    b_up(gb.at[slot_u], slot_u, 1, yu).start()
    b_down(gb.at[slot_u], slot_u, 1, yu).start()
    remote(gb.at[slot_o, lo], gb.at[slot_o, lo], sb, bh.at[0], y=yd).wait_recv()
    remote(gb.at[slot_o, hi], gb.at[slot_o, hi], sb, bh.at[1], y=yd).wait_recv()
    b_up(gb.at[slot_o], slot_o, 1, yo).start()
    b_down(gb.at[slot_o], slot_o, 1, yo).start()

    def side_forward(zz):
        sd, su = zz * NY + yd, zz * NY + yu
        remote(ga.at[sd], ga.at[sd], sa, ay.at[0, zz], y=yd).wait_recv()
        remote(ga.at[sd, lo], ga.at[sd, lo], sa, ah.at[0, zz], y=yu).start()
        remote(ga.at[su], ga.at[su], sa, ay.at[1, zz], y=yd).wait_recv()
        remote(ga.at[su, hi], ga.at[su, hi], sa, ah.at[1, zz], y=yd).start()

    half = NZ // 2

    def step(s, carry):
        z_lo, z_hi = mod(z - s, NZ), mod(z + s, NZ)
        slot = z_lo * NY + y
        a_up(ga.at[slot], slot, s).wait_recv()

        @pl.when(s < half)
        def _():
            a_up(ga.at[slot], slot, s + 1).start()

        a_side(ga.at[slot], z_lo)

        @pl.when(s < half)
        def _():
            slot2 = z_hi * NY + y
            a_down(ga.at[slot2], slot2, s).wait_recv()

            @pl.when(s < half - 1)
            def _():
                a_down(ga.at[slot2], slot2, s + 1).start()

            a_side(ga.at[slot2], z_hi)

        for j in (y, yd, yu, yo):
            sl = z_lo * NY + j
            b_up(gb.at[sl], sl, s, j).wait_recv()

            @pl.when(s < half)
            def _():
                b_up(gb.at[sl], sl, s + 1, j).start()

            @pl.when(s < half)
            def _():
                sl2 = z_hi * NY + j
                b_down(gb.at[sl2], sl2, s, j).wait_recv()

                @pl.when(s < half - 1)
                def _():
                    b_down(gb.at[sl2], sl2, s + 1, j).start()

        side_forward(mod(z - s + 1, NZ))

        @pl.when(s > 1)
        def _():
            side_forward(mod(z + s - 1, NZ))

        return carry

    lax.fori_loop(1, half + 1, step, 0)
    side_forward(mod(z + half, NZ))

    def finish(zz, carry):
        so = zz * NY + yo
        remote(ga.at[so, lo], ga.at[so, lo], sa, ah.at[0, zz], y=yd).wait_recv()
        remote(ga.at[so, hi], ga.at[so, hi], sa, ah.at[1, zz], y=yd).wait_recv()
        return carry

    lax.fori_loop(0, NZ, finish, 0)
    n = NZ * NY - 1
    every = pl.ds(0, n)
    remote(ga.at[every], ga.at[every], sa, az.at[0, 0], y=yd).wait_send()
    remote(gb.at[every], gb.at[every], sb, az.at[0, 0], y=yd).wait_send()


def gather_weights(a, b):
    n = NZ * NY
    dma = pltpu.SemaphoreType.DMA
    return pl.pallas_call(
        gather_body,
        name="gather_weights",
        out_shape=(
            jax.ShapeDtypeStruct((n,) + a.shape, BF16),
            jax.ShapeDtypeStruct((n,) + b.shape, BF16),
        ),
        in_specs=[pl.BlockSpec(memory_space=VMEM)] * 2,
        out_specs=[pl.BlockSpec(memory_space=VMEM)] * 2,
        scratch_shapes=[
            dma((2,)),
            dma((2, NZ // 2 + 1)),
            dma((2, NZ)),
            dma((2, NZ)),
            dma((2, NZ // 2 + 1, NY)),
            dma((2,)),
            dma((2,)),
        ],
        compiler_params=pltpu.CompilerParams(collective_id=0, has_side_effects=True),
    )(a, b)


def log1p_of(e):
    poly = e * (
        1.0
        + e * (-0.5 + e * (1 / 3 + e * (-0.25 + e * (0.2 + e * (-1 / 6 + e * (1 / 7))))))
    )
    return jnp.where(e < 0.0625, poly, jnp.log(1.0 + e))


def log_sigmoid(x):
    return jnp.minimum(x, 0.0) - log1p_of(jnp.exp(-jnp.abs(x)))


def split3(x):
    hi = x.astype(BF16).astype(F32)
    mid = (x - hi).astype(BF16).astype(F32)
    return hi, mid, x - hi - mid


def project_body(
    tok_ref, gain_ref, ga, gb, bias_ref, decay_ref, qkvo, aq, kv, pk, rows_ref, cols_ref, normed
):
    x = tok_ref[...].astype(F32)
    scale = lax.rsqrt(jnp.mean(x * x, axis=-1, keepdims=True) + EPS)
    normed[...] = (x * scale * gain_ref[...]).astype(BF16)
    gates = (
        jnp.dot(normed[...], gb[...].reshape(D, -1)[:, 0:128], preferred_element_type=F32)
        + bias_ref[...]
    )
    for c in range(3):
        out = jnp.dot(
            normed[...],
            ga[:, :, c * 256 : c * 256 + 256].reshape(D, 256),
            preferred_element_type=F32,
        ).astype(BF16)
        if c < 2:
            qkvo[:, c * 256 : c * 256 + 256] = out
        else:
            aq[...] = out[:, 0:128]
            kv[...] = out[:, 128:256]
    gt = jnp.transpose(gates)
    in_f, in_b = gt[0:1], gt[2:3]
    lf_f = log_sigmoid(gt[1:2]) + decay_ref[0:1]
    lf_b = log_sigmoid(gt[3:4]) + decay_ref[1:2]
    lane = lax.broadcasted_iota(jnp.int32, (1, TOK), 1)
    cum, rev = lf_f, lf_b
    k = 1
    while k < TOK:
        cum = cum + jnp.where(lane >= k, pltpu.roll(cum, k, 1), 0.0)
        rev = rev + jnp.where(lane < TOK - k, pltpu.roll(rev, TOK - k, 1), 0.0)
        k *= 2
    tot_f = jnp.max(jnp.where(lane == TOK - 1, cum, -jnp.inf), axis=1, keepdims=True)
    tot_b = jnp.max(jnp.where(lane == 0, rev, -jnp.inf), axis=1, keepdims=True)
    end_f = tot_f - cum + in_f
    end_b = tot_b - rev + in_b
    m_f = jnp.max(end_f, axis=1, keepdims=True)
    m_b = jnp.max(end_b, axis=1, keepdims=True)
    w_f, w_b = jnp.exp(end_f - m_f), jnp.exp(end_b - m_b)
    zero = jnp.zeros((2, TOK), F32)
    rows = jnp.concatenate([in_f, cum, in_b, rev, w_f, w_b, zero], axis=0)
    rows_ref[...] = rows
    cols = jnp.transpose(jnp.concatenate([rows, jnp.zeros((120, TOK), F32)], axis=0))
    cols_ref[...] = cols
    key = qkvo[:, 128:256]
    val = qkvo[:, 256:384].astype(F32)
    wide = (1, 128)
    tail = []
    mats = []
    norms = jnp.dot(rows.astype(BF16), key, preferred_element_type=F32)
    for c in (4, 5):
        wv = (cols[:, c : c + 1] * val).astype(BF16)
        mats.append(
            lax.dot_general(key, wv, (((0,), (0,)), ((), ())), preferred_element_type=F32)
        )
        tail.append(norms[c : c + 1])
    for v in (m_f, tot_f, m_b, tot_b):
        tail.extend(jnp.broadcast_to(p, wide) for p in split3(v))
    tail.append(jnp.zeros((2, 128), F32))
    last = jnp.concatenate(tail, axis=0).astype(BF16)
    for q in range(NY):
        pk[q, 0:32] = mats[0][q * 32 : q * 32 + 32].astype(BF16)
        pk[q, 32:64] = mats[1][q * 32 : q * 32 + 32].astype(BF16)
        pk[q, 64:80] = last


def project(tokens, gain, ga, gb, bias, decay):
    sds = jax.ShapeDtypeStruct
    return pl.pallas_call(
        project_body,
        name="project",
        out_shape=(
            sds((TOK, 512), BF16),
            sds((TOK, 128), BF16),
            sds((TOK, 128), BF16),
            sds((NY, 80, 128), BF16),
            sds((8, TOK), F32),
            sds((TOK, 128), F32),
        ),
        in_specs=[pl.BlockSpec(memory_space=VMEM)] * 6,
        out_specs=[pl.BlockSpec(memory_space=VMEM)] * 6,
        scratch_shapes=[pltpu.VMEM((TOK, D), BF16)],
    )(tokens, gain, ga, gb, bias, decay)


def step_state(state, piece):
    peak, mat, norm = state
    p_peak, p_decay, p_mat, p_norm = piece
    new = jnp.maximum(peak + p_decay, p_peak)
    old_s, new_s = jnp.exp(peak + p_decay - new), jnp.exp(p_peak - new)
    return new, mat * old_s + p_mat * new_s, norm * old_s + p_norm * new_s


def joined(tail, at):
    return tail[at : at + 1] + tail[at + 1 : at + 2] + tail[at + 2 : at + 3]


def scan_body(pk, kv, st, nm, halo, p1, zp, p2, p3, keep, s1, r1, s2, r2, s3, r3, sh, rh):
    z = lax.axis_index("z")
    y = lax.axis_index("y")
    me = z * NY + y
    nxt, prv = mod(me + 1, NZ * NY), mod(me - 1, NZ * NY)
    zn, yn = lax.div(nxt, NY), lax.rem(nxt, NY)
    zq, yq = lax.div(prv, NY), lax.rem(prv, NY)
    barrier = pltpu.get_barrier_semaphore()
    for d in range(1, NZ):
        pl.semaphore_signal(
            barrier, inc=1, device_id={"z": mod(z + d, NZ)}, device_id_type=MESH
        )
    for d in range(1, NY):
        pl.semaphore_signal(
            barrier, inc=1, device_id={"y": mod(y + d, NY)}, device_id_type=MESH
        )
    pl.semaphore_signal(barrier, inc=1, device_id={"z": zn, "y": yn}, device_id_type=MESH)
    pl.semaphore_signal(barrier, inc=1, device_id={"z": zq, "y": yq}, device_id_type=MESH)
    pl.semaphore_wait(barrier, NZ + NY)

    for d in (2, 1, 3):
        t = mod(y + d, NY)
        remote(pk.at[t], p1.at[y], s1.at[d - 1], r1.at[y], y=t).start()
    first, last = pl.ds(0, WINDOW), pl.ds(TOK - WINDOW, WINDOW)
    to_next = remote(kv.at[last], halo.at[0], sh.at[0], rh.at[0], z=zn, y=yn)
    to_prev = remote(kv.at[first], halo.at[1], sh.at[1], rh.at[1], z=zq, y=yq)
    to_next.start()
    to_prev.start()
    p1[y] = pk[y]
    for d in range(1, NY):
        t = mod(y + d, NY)
        remote(p1.at[t], p1.at[t], s1.at[0], r1.at[t], y=t).wait_recv()

    def local_piece(j, back):
        tail = p1[j, 64:80].astype(F32)
        if back:
            return joined(tail, 8), joined(tail, 11), p1[j, 32:64].astype(F32), tail[1:2]
        return joined(tail, 2), joined(tail, 5), p1[j, 0:32].astype(F32), tail[0:1]

    def empty():
        return (
            jnp.full((1, 128), FLOOR_LOG, F32),
            jnp.zeros((32, 128), F32),
            jnp.zeros((1, 128), F32),
        )

    for back in (0, 1):
        state, decay = empty(), jnp.zeros((1, 128), F32)
        for j in reversed(range(NY)) if back else range(NY):
            piece = local_piece(j, back)
            state = step_state(state, piece)
            decay = decay + piece[1]
        zp[back, 0:32] = state[1].astype(BF16)
        zp[back, 32:48] = jnp.concatenate(
            [state[2], *split3(state[0]), *split3(decay), jnp.zeros((9, 128), F32)], axis=0
        ).astype(BF16)
    for d in (8, 7, 9, 6, 10, 5, 11, 4, 12, 3, 13, 2, 14, 1, 15):
        t = mod(z + d, NZ)
        remote(
            zp.at[lax.div(z + d, NZ)], p2.at[z], s2.at[d - 1], r2.at[z], z=t
        ).start()
    for d in range(1, NZ):
        t = mod(z + d, NZ)
        remote(p2.at[t], p2.at[t], s2.at[0], r2.at[t], z=t).wait_recv()

    def far(i, state):
        tail = p2[i, 32:48].astype(F32)
        return step_state(
            state, (joined(tail, 1), joined(tail, 4), p2[i, 0:32].astype(F32), tail[0:1])
        )

    fwd = lax.fori_loop(0, z, far, empty())
    bwd = lax.fori_loop(0, NZ - 1 - z, lambda i, s: far(NZ - 1 - i, s), empty())
    for j in range(NY):
        p3[j, 0:32] = fwd[1].astype(BF16)
        keep[j, 0:1] = fwd[2]
        keep[j, 2:3] = fwd[0]
        fwd = step_state(fwd, local_piece(j, 0))
    for j in reversed(range(NY)):
        p3[j, 32:64] = bwd[1].astype(BF16)
        keep[j, 1:2] = bwd[2]
        keep[j, 3:4] = bwd[0]
        bwd = step_state(bwd, local_piece(j, 1))
    for d in (2, 1, 3):
        t = mod(y + d, NY)
        remote(p3.at[t], st.at[y], s3.at[d - 1], r3.at[y], y=t).start()
    st[y] = p3[y]
    nm[0:4] = keep[y, 0:4]
    nm[4:8] = jnp.zeros((4, 128), F32)
    for d in range(1, NY):
        t = mod(y + d, NY)
        remote(st.at[t], st.at[t], s3.at[0], r3.at[t], y=t).wait_recv()
    to_next.wait_recv()
    to_prev.wait_recv()
    for d in range(1, NY):
        remote(pk.at[0], p1.at[0], s1.at[d - 1], r1.at[0], y=y).wait_send()
        remote(p3.at[0], st.at[0], s3.at[d - 1], r3.at[0], y=y).wait_send()
    for d in range(1, NZ):
        remote(zp.at[0], p2.at[0], s2.at[d - 1], r2.at[0], z=z).wait_send()
    to_next.wait_send()
    to_prev.wait_send()


def scan_states(pk, kv):
    sds = jax.ShapeDtypeStruct
    dma = pltpu.SemaphoreType.DMA
    return pl.pallas_call(
        scan_body,
        name="scan_states",
        out_shape=(
            sds((NY, 64, 128), BF16),
            sds((8, 128), F32),
            sds((2, WINDOW, 128), BF16),
        ),
        in_specs=[pl.BlockSpec(memory_space=VMEM)] * 2,
        out_specs=[pl.BlockSpec(memory_space=VMEM)] * 3,
        scratch_shapes=[
            pltpu.VMEM((NY, 80, 128), BF16),
            pltpu.VMEM((2, 48, 128), BF16),
            pltpu.VMEM((NZ, 48, 128), BF16),
            pltpu.VMEM((NY, 64, 128), BF16),
            pltpu.VMEM((NY, 8, 128), F32),
            dma((NY - 1,)),
            dma((NY,)),
            dma((NZ - 1,)),
            dma((NZ,)),
            dma((NY - 1,)),
            dma((NY,)),
            dma((2,)),
            dma((2,)),
        ],
        compiler_params=pltpu.CompilerParams(collective_id=1, has_side_effects=True),
    )(pk, kv)


def mix_body(qkvo, aq, kv, rows_ref, cols_ref, st, nm, halo, mgain, sink, mix, logs, win):
    z = lax.axis_index("z")
    y = lax.axis_index("y")
    me = z * NY + y
    query, key, value = qkvo[:, 0:128], qkvo[:, 128:256], qkvo[:, 256:384]
    scale = M_DIM**-0.5
    across = (((1,), (1,)), ((), ()))
    dots = lax.dot_general(query, key, across, preferred_element_type=F32) * scale
    ti = lax.broadcasted_iota(jnp.int32, (TOK, TOK), 0)
    si = lax.broadcasted_iota(jnp.int32, (TOK, TOK), 1)
    qf = query.astype(F32) * scale
    total = None
    for back in (0, 1):
        ins = rows_ref[2 * back : 2 * back + 1]
        cum = rows_ref[2 * back + 1 : 2 * back + 2]
        cum_t = cols_ref[:, 2 * back + 1 : 2 * back + 2]
        keep = (si >= ti) if back else (si <= ti)
        log_w = jnp.where(keep, cum_t + (ins - cum), -jnp.inf)
        inter = cum_t + nm[2 + back : 3 + back, 0:1]
        top = jnp.maximum(inter, jnp.max(log_w, axis=1, keepdims=True))
        scores = dots * jnp.exp(log_w - top)
        w_inter = jnp.exp(inter - top)
        mat = st[:, 32 * back : 32 * back + 32].reshape(128, 128)
        numer = jnp.dot(scores.astype(BF16), value, preferred_element_type=F32) + (
            w_inter * scale
        ) * jnp.dot(query, mat, preferred_element_type=F32)
        denom = jnp.sum(scores, axis=1, keepdims=True) + w_inter * jnp.sum(
            qf * nm[back : back + 1], axis=1, keepdims=True
        )
        part = numer / jnp.maximum(jnp.abs(denom), jnp.exp(-top))
        total = part if total is None else total + part
    gate = qkvo[:, 384:512].astype(F32)
    u = total / (1.0 + jnp.exp(-gate))
    norm = lax.rsqrt(jnp.mean(u * u, axis=1, keepdims=True) + EPS)
    mix[:, 0:128] = (u * norm * mgain[...]).astype(BF16)

    win[0:WINDOW] = halo[0]
    win[WINDOW : WINDOW + TOK] = kv[...]
    win[WINDOW + TOK :] = halo[1]
    lane = lax.broadcasted_iota(jnp.int32, (WINDOW, 128), 1)
    two = lax.broadcasted_iota(jnp.int32, (2 * WINDOW, 3 * WINDOW), 0)
    col = lax.broadcasted_iota(jnp.int32, (2 * WINDOW, 3 * WINDOW), 1)
    head = two >= WINDOW
    off = col - jnp.where(head, two - WINDOW, two)
    in_window = (off >= 0) & (off <= 2 * WINDOW)
    head_row = lax.broadcasted_iota(jnp.int32, (2 * WINDOW, 1), 0) >= WINDOW
    sink_col = jnp.where(head_row, sink[0:1, 1:2], sink[0:1, 0:1])
    for b in range(2):
        qb = aq[b * WINDOW : b * WINDOW + WINDOW].astype(F32)
        q0 = jnp.where(lane < W_DIM, qb, 0.0)
        q1 = jnp.where(lane < W_DIM, pltpu.roll(qb, W_DIM, 1), 0.0)
        qq = jnp.concatenate([q0, q1], axis=0).astype(BF16)
        keys = win[b * WINDOW : b * WINDOW + 3 * WINDOW]
        scores = lax.dot_general(qq, keys, across, preferred_element_type=F32) * W_DIM**-0.5
        place = me * TOK + (b - 1) * WINDOW + col
        usable = in_window & (place >= 0) & (place < NZ * NY * TOK)
        scores = jnp.where(usable, scores, -jnp.inf)
        peak = jnp.maximum(sink_col, jnp.max(scores, axis=1, keepdims=True))
        weights = jnp.exp(scores - peak)
        tot = jnp.exp(sink_col - peak) + jnp.sum(weights, axis=1, keepdims=True)
        out = jnp.dot(weights.astype(BF16), keys, preferred_element_type=F32) / tot
        o0 = pltpu.roll(out[0:WINDOW], W_DIM, 1)
        o1 = out[WINDOW:]
        mix[b * WINDOW : b * WINDOW + WINDOW, 128:256] = jnp.where(
            lane < W_DIM, o0, o1
        ).astype(BF16)
        logt = jnp.transpose(jnp.broadcast_to(peak + jnp.log(tot), (2 * WINDOW, 128)))
        logs[0:1, b * WINDOW : b * WINDOW + WINDOW] = logt[0:1, 0:WINDOW]
        logs[1:2, b * WINDOW : b * WINDOW + WINDOW] = logt[0:1, WINDOW:]


def mix_local(*args):
    sds = jax.ShapeDtypeStruct
    return pl.pallas_call(
        mix_body,
        name="mix",
        out_shape=(sds((TOK, 256), BF16), sds((2, TOK), F32)),
        in_specs=[pl.BlockSpec(memory_space=VMEM)] * len(args),
        out_specs=[pl.BlockSpec(memory_space=VMEM)] * 2,
        scratch_shapes=[pltpu.VMEM((TOK + 2 * WINDOW, 128), BF16)],
    )(*args)


def heads_body(mix, full, ssem, rx, rh, rc):
    t = lax.axis_index("tp")
    x, c = lax.div(t, 2), lax.rem(t, 2)
    o = 1 - c
    xu, xd, xo = mod(x + 1, 4), mod(x - 1, 4), mod(x + 2, 4)
    partner, up, down = 2 * x + o, 2 * xu + c, 2 * xd + c
    far = 2 * xo + c
    barrier = pltpu.get_barrier_semaphore()
    for p in (partner, up, down):
        pl.semaphore_signal(barrier, inc=1, device_id={"tp": p}, device_id_type=MESH)
    pl.semaphore_wait(barrier, 3)
    lo, hi = pl.ds(0, TOK // 2), pl.ds(TOK // 2, TOK // 2)
    remote(mix, full.at[t], ssem, rx.at[0], tp=up).start()
    remote(mix, full.at[t], ssem, rx.at[1], tp=down).start()
    remote(mix, full.at[t], ssem, rc.at[0], tp=partner).start()
    full[t] = mix[...]
    remote(mix, full.at[down], ssem, rx.at[0], tp=up).wait_recv()
    remote(full.at[down, lo], full.at[down, lo], ssem, rh.at[0], tp=up).start()
    remote(full.at[down], full.at[down], ssem, rc.at[1], tp=partner).start()
    remote(mix, full.at[up], ssem, rx.at[1], tp=up).wait_recv()
    remote(full.at[up, hi], full.at[up, hi], ssem, rh.at[1], tp=down).start()
    remote(full.at[up], full.at[up], ssem, rc.at[2], tp=partner).start()
    remote(full.at[far, lo], full.at[far, lo], ssem, rh.at[0], tp=up).wait_recv()
    remote(full.at[far, lo], full.at[far, lo], ssem, rc.at[3], tp=partner).start()
    remote(full.at[far, hi], full.at[far, hi], ssem, rh.at[1], tp=up).wait_recv()
    remote(full.at[far, hi], full.at[far, hi], ssem, rc.at[4], tp=partner).start()
    remote(mix, full.at[partner], ssem, rc.at[0], tp=partner).wait_recv()
    remote(mix, full.at[2 * xd + o], ssem, rc.at[1], tp=partner).wait_recv()
    remote(mix, full.at[2 * xu + o], ssem, rc.at[2], tp=partner).wait_recv()
    other = 2 * xo + o
    remote(full.at[other, lo], full.at[other, lo], ssem, rc.at[3], tp=partner).wait_recv()
    remote(full.at[other, hi], full.at[other, hi], ssem, rc.at[4], tp=partner).wait_recv()
    every = pl.ds(0, NT - 1)
    remote(full.at[every], full.at[every], ssem, rc.at[0], tp=partner).wait_send()


def gather_heads(mix):
    dma = pltpu.SemaphoreType.DMA
    return pl.pallas_call(
        heads_body,
        name="gather_heads",
        out_shape=jax.ShapeDtypeStruct((NT, TOK, 256), BF16),
        in_specs=[pl.BlockSpec(memory_space=VMEM)],
        out_specs=pl.BlockSpec(memory_space=VMEM),
        scratch_shapes=[dma, dma((2,)), dma((2,)), dma((5,))],
        compiler_params=pltpu.CompilerParams(collective_id=2, has_side_effects=True),
    )(mix)


def last_body(full, gb, out):
    acc = None
    for t in range(NT):
        for part in (0, 1):
            w = gb[8 * t : 8 * t + 8, 16 * part : 16 * part + 16, 128:384].reshape(128, 256)
            term = jnp.dot(
                full[t, :, 128 * part : 128 * part + 128], w, preferred_element_type=F32
            )
            acc = term if acc is None else acc + term
    out[...] = acc.astype(BF16)


def project_out(full, gb):
    return pl.pallas_call(
        last_body,
        name="project_out",
        out_shape=jax.ShapeDtypeStruct((TOK, 256), BF16),
        in_specs=[pl.BlockSpec(memory_space=VMEM)] * 2,
        out_specs=pl.BlockSpec(memory_space=VMEM),
    )(full, gb)


def on_device(
    tokens,
    input_norm_gain,
    mq_weight,
    mk_weight,
    mv_weight,
    mo_weight,
    gate_weight,
    gate_bias,
    decay_extra,
    m_gain,
    aq_weight,
    ak_weight,
    av_weight,
    sink_logit,
    out_m_weight,
    out_a_weight,
):
    a = jnp.concatenate(
        [mq_weight, mk_weight, mv_weight, mo_weight, aq_weight, ak_weight, av_weight], axis=1
    )
    gate = jnp.pad(gate_weight[:, :, 0], ((0, 0), (0, 124)))
    b = jnp.concatenate(
        [gate, jnp.concatenate([out_m_weight, out_a_weight], axis=0)], axis=1
    )
    ga, gb = gather_weights(a, b)
    bias = jnp.pad(gate_bias.T, ((0, 0), (0, 124)))
    qkvo, aq, kv, pk, rows, cols = project(
        tokens, input_norm_gain[None], ga, gb, bias, decay_extra[:, 0]
    )
    st, nm, halo = scan_states(pk, kv)
    mix, logs = mix_local(
        qkvo, aq, kv, rows, cols, st, nm, halo, m_gain[None], sink_logit[None]
    )
    full = gather_heads(mix)
    return project_out(full, gb), logs


def solution(mesh):
    split = Mesh(mesh.devices.reshape(NZ, NY, NT), ("z", "y", "tp"))
    return jax.shard_map(
        on_device,
        mesh=split,
        in_specs=(
            P(SP, None),
            P(),
            P(SP, "tp"),
            P(SP, "tp"),
            P(SP, "tp"),
            P(SP, "tp"),
            P(SP, None, "tp"),
            P(None, "tp"),
            P(None, "tp", SP),
            P("tp"),
            P(SP, "tp"),
            P(SP, "tp"),
            P(SP, "tp"),
            P("tp"),
            P(SP, "tp"),
            P(SP, "tp"),
        ),
        out_specs=(P(SP, "tp"), P("tp", SP)),
        check_vma=False,
    )
```

time: 499 us -> 113 us (0.23)
  the two profiles are of different devices: /device:TPU:6 before, /device:TPU:1 now
where the time goes in v1:
time: 113 us
  Pallas kernels  106 us (94%)
  local copies, waits for them, and re-layouts  4.78 us (4%)
  other arithmetic  1.32 us (1%)
    pallas_call x1, Pallas kernels, gather_weights(): pl.pallas_call(gather_body, name='gather_weights', out_shape=(jax.ShapeDt...  48.9 us
    pallas_call x1, Pallas kernels, gather_heads(): pl.pallas_call(heads_body, name='gather_heads', out_shape=jax.ShapeDtypeS...  22.9 us
    pallas_call x1, Pallas kernels, scan_states(): pl.pallas_call(scan_body, name='scan_states', out_shape=(sds((NY, 64, 128...  21.9 us
    pallas_call x1, Pallas kernels, project(): pl.pallas_call(project_body, name='project', out_shape=(sds((TOK, 512), B...  5.32 us
    pallas_call x1, Pallas kernels, mix_local(): pl.pallas_call(mix_body, name='mix', out_shape=(sds((TOK, 256), BF16), sd...  4.02 us
    pallas_call x1, Pallas kernels, project_out(): pl.pallas_call(last_body, name='project_out', out_shape=jax.ShapeDtypeStr...  3.07 us

profile of v1, /device:TPU:1, one launch (start us, length us, event | category | flops | bytes accessed | tf_op | source)
XLA Modules:
  0.0 112.9 jit_solution(18029394037223975291)
XLA Ops:
  0.6 1.2 %pad.9.bias_ref = f32[1,128]{1,0:T(1,128)} pad(f32[1,4]{1,0:T(1,128)} %bitcast.13, f32[]{:T(128)} %constant.4.clone.1), padding=0_0x0_124 | pad | bytes 532 | tf_op jit(solution)/shard_map/jit(_pad)/pad | solution.py:628
  1.9 1.3 %copy.21 = f32[2,1,256]{2,0,1:T(2,128)} copy(f32[2,1,256]{2,1,0:T(1,128)} %param.24) | data formatting | bytes 4096
  3.1 0.8 copy.18
  3.9 1.3 %fusion.1.b_ref = bf16[32,384]{1,0:T(8,128)(2,1)} fusion(bf16[32,4]{1,0:T(8,128)(2,1)S(1)} %copy.18, bf16[16,256]{1,0:T(8,128)(2,1)} %param.31, bf16[16,256]{1,0:T(8,128)(2,1)} %param.30), kind=kLoop, calls=%fused_computation.2 | loop fusion | flops 98304 | bytes 41216 | tf_op jit(solution)/shard_map/concatenate | solution.py:624
  5.2 1.5 %concatenate.9.a_ref = bf16[32,768]{1,0:T(8,128)(2,1)} concatenate(bf16[32,128]{1,0:T(8,128)(2,1)} %param.18, bf16[32,128]{1,0:T(8,128)(2,1)} %param.19, bf16[32,128]{1,0:T(8,128)(2,1)} %param.20, bf16[32,128]{1,0:T(8,128)(2,1)} %param.21, bf16[32,128]{1,0:T(8,128)(2,1)} %param.26, bf16[32,64]{1,0:T(8,128)(2,1)} %param.27, bf16[32,64]{1,0:T(8,128)(2,1)} %param.28), dimensions={1} | concatenate | bytes 98304 | tf_op jit(solution)/shard_map/concatenate | solution.py:620
  6.7 48.9 %gather_weights.1 = (bf16[64,32,768]{2,1,0:T(8,128)(2,1)}, bf16[64,32,384]{2,1,0:T(8,128)(2,1)}) custom-call(bf16[32,768]{1,0:T(8,128)(2,1)} %concatenate.9.a_ref, bf16[32,384]{1,0:T(8,128)(2,1)} %fusion.1.b_ref), custom_call_target="tpu_custom_call" | custom-call | tf_op jit(solution)/shard_map/gather_weights/pallas_call | solution.py:176
  55.7 5.3 %project.1 = (bf16[256,512]{1,0:T(8,128)(2,1)}, bf16[256,128]{1,0:T(8,128)(2,1)}, bf16[256,128]{1,0:T(8,128)(2,1)}, bf16[4,80,128]{2,1,0:T(8,128)(2,1)}, f32[8,256]{1,0:T(8,128)}, /*index=5*/f32[256,128]{1,0:T(8,128)}) custom-call(bf16[256,2048]{1,0:T(8,128)(2,1)} %tok_ref.1, f32[1,2048]{1,0:T(1,128)} %bitcast.8, bf16[64,32,768]{2,1,0:T(8,128)(2,1)} %get-tuple-element.15.ga, ...), custom_call_target="tpu_custom_call" | custom-call | tf_op jit(solution)/shard_map/project/pallas_call | solution.py:284
  61.0 21.9 %scan_states.1 = (bf16[4,64,128]{2,1,0:T(8,128)(2,1)}, f32[8,128]{1,0:T(8,128)}, bf16[2,128,128]{2,1,0:T(8,128)(2,1)}) custom-call(bf16[4,80,128]{2,1,0:T(8,128)(2,1)} %get-tuple-element.22.pk, bf16[256,128]{1,0:T(8,128)(2,1)} %get-tuple-element.19.kv), custom_call_target="tpu_custom_call" | custom-call | tf_op jit(solution)/shard_map/scan_states/pallas_call | solution.py:419
  82.9 4.0 %mix.1 = (bf16[256,256]{1,0:T(8,128)(2,1)}, f32[2,256]{1,0:T(2,128)}) custom-call(bf16[256,512]{1,0:T(8,128)(2,1)} %get-tuple-element.17.qkvo, bf16[256,128]{1,0:T(8,128)(2,1)} %get-tuple-element.18.aq, bf16[256,128]{1,0:T(8,128)(2,1)} %get-tuple-element.19.kv, f32[8,256]{1,0:T(8,128)} %get-tuple-element.20.rows_ref, f32[256,128]{1,0:T(8,128)} %get-tuple-element.21.cols_ref, ...), custom_call_target="tpu_custom_call" | custom-call | tf_op jit(solution)/shard_map/mix/pallas_call | solution.py:521
  86.9 22.9 %gather_heads.1.full = bf16[8,256,256]{2,1,0:T(8,128)(2,1)} custom-call(bf16[256,256]{1,0:T(8,128)(2,1)} %get-tuple-element.26.mix), custom_call_target="tpu_custom_call" | custom-call | tf_op jit(solution)/shard_map/gather_heads/pallas_call | solution.py:569
  109.8 3.1 %project_out.1 = bf16[256,256]{1,0:T(8,128)(2,1)} custom-call(bf16[8,256,256]{2,1,0:T(8,128)(2,1)} %gather_heads.1.full, bf16[64,32,384]{2,1,0:T(8,128)(2,1)} %get-tuple-element.16.gb), custom_call_target="tpu_custom_call" | custom-call | tf_op jit(solution)/shard_map/project_out/pallas_call | solution.py:593

commit v2 on v1

v2 whole, which is shorter than its diff:
```python
import jax
import jax.numpy as jnp
from jax import lax
from jax.experimental import pallas as pl
from jax.experimental.pallas import tpu as pltpu
from jax.sharding import Mesh
from jax.sharding import PartitionSpec as P

M_DIM = 128
W_DIM = 64
WINDOW = 128
EPS = 1e-06
FLOOR_LOG = -1e30
NZ = 16
NY = 4
NX = 4
NT = 8
TOK = 256
D = 2048
HALF = NZ // 2
A_COLS = 640
B_ROWS = 104
SP = ("z", "y")
MESH = pl.DeviceIdType.MESH
F32 = jnp.float32
BF16 = jnp.bfloat16
ACROSS = (((1,), (1,)), ((), ()))


def mod(a, n):
    return lax.rem(a + n, n)


def remote(src, dst, ssem, rsem, **where):
    return pltpu.make_async_remote_copy(
        src_ref=src,
        dst_ref=dst,
        send_sem=ssem,
        recv_sem=rsem,
        device_id=where,
        device_id_type=MESH,
    )


def log1p_of(e):
    poly = e * (
        1.0
        + e * (-0.5 + e * (1 / 3 + e * (-0.25 + e * (0.2 + e * (-1 / 6 + e * (1 / 7))))))
    )
    return jnp.where(e < 0.0625, poly, jnp.log(1.0 + e))


def log_sigmoid(x):
    return jnp.minimum(x, 0.0) - log1p_of(jnp.exp(-jnp.abs(x)))


def split3(x):
    hi = x.astype(BF16).astype(F32)
    mid = (x - hi).astype(BF16).astype(F32)
    return hi, mid, x - hi - mid


def joined(tail, at):
    return tail[at : at + 1] + tail[at + 1 : at + 2] + tail[at + 2 : at + 3]


def step_state(state, piece):
    peak, mat, norm = state
    p_peak, p_decay, p_mat, p_norm = piece
    new = jnp.maximum(peak + p_decay, p_peak)
    old_s, new_s = jnp.exp(peak + p_decay - new), jnp.exp(p_peak - new)
    return new, mat * old_s + p_mat * new_s, norm * old_s + p_norm * new_s


def empty_state():
    return (
        jnp.full((1, 128), FLOOR_LOG, F32),
        jnp.zeros((32, 128), F32),
        jnp.zeros((1, 128), F32),
    )


def layer_body(
    tok_hbm,
    gain,
    mq,
    mk,
    mv,
    mo,
    gate_t,
    bias,
    decay,
    mgain,
    aq_w,
    ak_w,
    av_w,
    sink,
    om,
    oa,
    out,
    logs,
    tok,
    wa,
    wb,
    ga,
    gb,
    normed,
    acc_a,
    acc_b,
    qkvo,
    aq,
    kv,
    halo,
    win,
    pk,
    p1,
    zp,
    p2,
    p3,
    st,
    keep,
    mixes,
    full,
    local_sem,
    ssem,
    az,
    ay,
    ah,
    bz,
    by,
    bh,
    s1,
    r1,
    s2,
    r2,
    s3,
    r3,
    sh,
    rh,
    hs,
    hx,
    hh,
    hc,
):
    z = lax.axis_index("z")
    y = lax.axis_index("y")
    t = lax.axis_index("tp")
    me = z * NY + y
    zu, zd = mod(z + 1, NZ), mod(z - 1, NZ)
    yu, yd = mod(y + 1, NY), mod(y - 1, NY)
    yo = mod(y + 2, NY)
    nxt, prv = mod(me + 1, NZ * NY), mod(me - 1, NZ * NY)
    zn, yn = lax.div(nxt, NY), lax.rem(nxt, NY)
    zq, yq = lax.div(prv, NY), lax.rem(prv, NY)
    x, c = lax.div(t, 2), lax.rem(t, 2)
    o = 1 - c
    xu, xd, xo = mod(x + 1, NX), mod(x - 1, NX), mod(x + 2, NX)
    partner, t_up, t_down, t_far = 2 * x + o, 2 * xu + c, 2 * xd + c, 2 * xo + c

    loads = []

    def load(src, dst):
        copy = pltpu.make_async_copy(src, dst, local_sem.at[len(loads)])
        copy.start()
        loads.append(copy)

    for i, w in enumerate((mq, mk, mv, mo, aq_w)):
        load(w, wa.at[:, 128 * i : 128 * i + 128])
    for i, w in enumerate((om, oa)):
        for part in (0, 1):
            at = 32 + 32 * i + 16 * part
            load(w.at[:, 128 * part : 128 * part + 128], wb.at[at : at + 16])
    load(tok_hbm, tok)
    barrier = pltpu.get_barrier_semaphore()
    hello = [{"z": zu}, {"z": zd}, {"y": yu}, {"y": yd}, {"y": yo}]
    hello += [{"z": zn, "y": yn}, {"z": zq, "y": yq}]
    hello += [{"tp": partner}, {"tp": t_up}, {"tp": t_down}]
    for where in hello:
        pl.semaphore_signal(barrier, inc=1, device_id=where, device_id_type=MESH)
    wb[0:32] = jnp.concatenate([ak_w[...], av_w[...]], axis=1)
    gate_rows = jnp.concatenate([gate_t[...].astype(F32), jnp.zeros((4, 96), F32)], axis=1)
    gate_row = gate_rows[0:1]
    for g in range(1, 4):
        gate_row = gate_row + pltpu.roll(gate_rows[g : g + 1], 32 * g, 1)
    wb[96:104] = jnp.concatenate([gate_row, jnp.zeros((7, 128), F32)], axis=0).astype(BF16)
    for copy in loads[:-1]:
        copy.wait()
    pl.semaphore_wait(barrier, len(hello))

    sa, sb = ssem.at[0], ssem.at[1]

    def a_up(src, slot, s):
        return remote(src, ga.at[slot], sa, az.at[0, s], z=zu)

    def a_down(src, slot, s):
        return remote(src, ga.at[slot], sa, az.at[1, s], z=zd)

    def a_side(src, zz):
        slot = zz * NY + y
        remote(src, ga.at[slot], sa, ay.at[0, zz], y=yu).start()
        remote(src, ga.at[slot], sa, ay.at[1, zz], y=yd).start()

    def b_up(src, slot, s, j):
        return remote(src, gb.at[slot], sb, bz.at[0, s, j], z=zu)

    def b_down(src, slot, s, j):
        return remote(src, gb.at[slot], sb, bz.at[1, s, j], z=zd)

    remote(wb, gb.at[me], sb, by.at[0], y=yu).start()
    remote(wb, gb.at[me], sb, by.at[1], y=yd).start()
    a_up(wa, me, 1).start()
    a_down(wa, me, 1).start()
    b_up(wb, me, 1, y).start()
    b_down(wb, me, 1, y).start()
    a_side(wa, z)
    ga[me] = wa[...]
    gb[me] = wb[...]

    loads[-1].wait()
    xs = tok[...].astype(F32)
    xs = xs * lax.rsqrt(jnp.mean(xs * xs, axis=-1, keepdims=True) + EPS) * gain[...]
    for i in range(NZ):
        normed[i] = xs[:, 128 * i : 128 * i + 128].astype(BF16)
    acc_a[...] = jnp.zeros_like(acc_a)
    acc_b[...] = jnp.zeros_like(acc_b)

    slot_d, slot_u, slot_o = z * NY + yd, z * NY + yu, z * NY + yo
    lo, hi = pl.ds(0, 16), pl.ds(16, 16)
    blo, bhi = pl.ds(0, 48), pl.ds(48, 56)
    remote(wb, gb.at[slot_d], sb, by.at[0], y=yd).wait_recv()
    remote(gb.at[slot_d, blo], gb.at[slot_d, blo], sb, bh.at[0], y=yu).start()
    b_up(gb.at[slot_d], slot_d, 1, yd).start()
    b_down(gb.at[slot_d], slot_d, 1, yd).start()
    remote(wb, gb.at[slot_u], sb, by.at[1], y=yd).wait_recv()
    remote(gb.at[slot_u, bhi], gb.at[slot_u, bhi], sb, bh.at[1], y=yd).start()
    b_up(gb.at[slot_u], slot_u, 1, yu).start()
    b_down(gb.at[slot_u], slot_u, 1, yu).start()
    remote(gb.at[slot_o, blo], gb.at[slot_o, blo], sb, bh.at[0], y=yd).wait_recv()
    remote(gb.at[slot_o, bhi], gb.at[slot_o, bhi], sb, bh.at[1], y=yd).wait_recv()
    b_up(gb.at[slot_o], slot_o, 1, yo).start()
    b_down(gb.at[slot_o], slot_o, 1, yo).start()

    def side_forward(zz):
        sd, su = zz * NY + yd, zz * NY + yu
        remote(ga.at[sd], ga.at[sd], sa, ay.at[0, zz], y=yd).wait_recv()
        remote(ga.at[sd, lo], ga.at[sd, lo], sa, ah.at[0, zz], y=yu).start()
        remote(ga.at[su], ga.at[su], sa, ay.at[1, zz], y=yd).wait_recv()
        remote(ga.at[su, hi], ga.at[su, hi], sa, ah.at[1, zz], y=yd).start()

    spread = lax.broadcasted_iota(jnp.int32, (32, 128), 0) == lax.rem(
        lax.broadcasted_iota(jnp.int32, (32, 128), 1), 32
    )

    def level(zz):
        so = zz * NY + yo
        remote(ga.at[so, lo], ga.at[so, lo], sa, ah.at[0, zz], y=yd).wait_recv()
        remote(ga.at[so, hi], ga.at[so, hi], sa, ah.at[1, zz], y=yd).wait_recv()
        rows = normed[zz]
        first = zz * NY
        for at, width in ((0, 256), (256, 256), (512, 128)):
            w = jnp.concatenate(
                [ga[first + j, :, at : at + width] for j in range(NY)], axis=0
            )
            acc_a[:, at : at + width] += jnp.dot(rows, w, preferred_element_type=F32)
        w = jnp.concatenate([gb[first + j, 0:32] for j in range(NY)], axis=0)
        g = jnp.concatenate(
            [
                jnp.where(spread, gb[first + j, 96:104].astype(F32)[0:1], 0.0).astype(BF16)
                for j in range(NY)
            ],
            axis=0,
        )
        acc_b[...] += jnp.dot(
            rows, jnp.concatenate([w, g], axis=1), preferred_element_type=F32
        )

    def both(d, what):
        what(mod(z - d, NZ))

        @pl.when((d > 0) & (d < HALF))
        def _():
            what(mod(z + d, NZ))

    def step(s, carry):
        z_lo, z_hi = mod(z - s, NZ), mod(z + s, NZ)
        slot = z_lo * NY + y
        a_up(ga.at[slot], slot, s).wait_recv()

        @pl.when(s < HALF)
        def _():
            a_up(ga.at[slot], slot, s + 1).start()

        a_side(ga.at[slot], z_lo)

        @pl.when(s < HALF)
        def _():
            slot2 = z_hi * NY + y
            a_down(ga.at[slot2], slot2, s).wait_recv()

            @pl.when(s < HALF - 1)
            def _():
                a_down(ga.at[slot2], slot2, s + 1).start()

            a_side(ga.at[slot2], z_hi)

        for j in (y, yd, yu, yo):
            sl = z_lo * NY + j
            b_up(gb.at[sl], sl, s, j).wait_recv()

            @pl.when(s < HALF)
            def _():
                b_up(gb.at[sl], sl, s + 1, j).start()

            @pl.when(s < HALF)
            def _():
                sl2 = z_hi * NY + j
                b_down(gb.at[sl2], sl2, s, j).wait_recv()

                @pl.when(s < HALF - 1)
                def _():
                    b_down(gb.at[sl2], sl2, s + 1, j).start()

        @pl.when(s >= 2)
        def _():
            both(s - 2, side_forward)

        @pl.when(s >= 4)
        def _():
            both(s - 4, level)

        return carry

    lax.fori_loop(1, HALF + 1, step, 0)

    def tail_step(d, carry):
        @pl.when(d < HALF + 1)
        def _():
            both(d, side_forward)

        both(d - 2, level)
        return carry

    lax.fori_loop(HALF - 1, HALF + 3, tail_step, 0)

    qkvo[...] = acc_a[:, 0:512].astype(BF16)
    aq[...] = acc_a[:, 512:640].astype(BF16)
    kv[...] = acc_b[:, 0:128].astype(BF16)
    first, last = pl.ds(0, WINDOW), pl.ds(TOK - WINDOW, WINDOW)
    to_next = remote(kv.at[last], halo.at[0], sh.at[0], rh.at[0], z=zn, y=yn)
    to_prev = remote(kv.at[first], halo.at[1], sh.at[1], rh.at[1], z=zq, y=yq)
    gt = jnp.sum(jnp.transpose(acc_b[:, 128:256]).reshape(4, 32, TOK), axis=1)
    in_f, in_b = gt[0:1] + bias[0:1, 0:1], gt[2:3] + bias[0:1, 2:3]
    lf_f = log_sigmoid(gt[1:2] + bias[0:1, 1:2]) + decay[0]
    lf_b = log_sigmoid(gt[3:4] + bias[0:1, 3:4]) + decay[1]
    to_next.start()
    to_prev.start()
    lane = lax.broadcasted_iota(jnp.int32, (1, TOK), 1)
    cum, rev = lf_f, lf_b
    k = 1
    while k < TOK:
        cum = cum + jnp.where(lane >= k, pltpu.roll(cum, k, 1), 0.0)
        rev = rev + jnp.where(lane < TOK - k, pltpu.roll(rev, TOK - k, 1), 0.0)
        k *= 2
    tot_f = jnp.max(jnp.where(lane == TOK - 1, cum, -jnp.inf), axis=1, keepdims=True)
    tot_b = jnp.max(jnp.where(lane == 0, rev, -jnp.inf), axis=1, keepdims=True)
    end_f = tot_f - cum + in_f
    end_b = tot_b - rev + in_b
    m_f = jnp.max(end_f, axis=1, keepdims=True)
    m_b = jnp.max(end_b, axis=1, keepdims=True)
    w_f, w_b = jnp.exp(end_f - m_f), jnp.exp(end_b - m_b)
    rows = jnp.concatenate([in_f, cum, in_b, rev, w_f, w_b, jnp.zeros((2, TOK), F32)], axis=0)
    cols = jnp.transpose(jnp.concatenate([rows, jnp.zeros((120, TOK), F32)], axis=0))
    query, key, value = qkvo[:, 0:128], qkvo[:, 128:256], qkvo[:, 256:384]
    val = value.astype(F32)
    tail, mats = [], []
    norms = jnp.dot(rows.astype(BF16), key, preferred_element_type=F32)
    for i in (4, 5):
        wv = (cols[:, i : i + 1] * val).astype(BF16)
        mats.append(
            lax.dot_general(key, wv, (((0,), (0,)), ((), ())), preferred_element_type=F32)
        )
        tail.append(norms[i : i + 1])
    for v in (m_f, tot_f, m_b, tot_b):
        tail.extend(jnp.broadcast_to(p, (1, 128)) for p in split3(v))
    tail.append(jnp.zeros((2, 128), F32))
    summary_tail = jnp.concatenate(tail, axis=0).astype(BF16)
    for q in range(NY):
        pk[q, 0:32] = mats[0][q * 32 : q * 32 + 32].astype(BF16)
        pk[q, 32:64] = mats[1][q * 32 : q * 32 + 32].astype(BF16)
        pk[q, 64:80] = summary_tail

    for d in (2, 1, 3):
        j = mod(y + d, NY)
        remote(pk.at[j], p1.at[y], s1.at[d - 1], r1.at[y], y=j).start()
    p1[y] = pk[y]

    scale = M_DIM**-0.5
    dots = lax.dot_general(query, key, ACROSS, preferred_element_type=F32) * scale
    ti = lax.broadcasted_iota(jnp.int32, (TOK, TOK), 0)
    si = lax.broadcasted_iota(jnp.int32, (TOK, TOK), 1)
    inside = []
    for back in (0, 1):
        cum_t = cols[:, 2 * back + 1 : 2 * back + 2]
        log_in = rows[2 * back : 2 * back + 1] - rows[2 * back + 1 : 2 * back + 2]
        usable = (si >= ti) if back else (si <= ti)
        log_w = jnp.where(usable, cum_t + log_in, -jnp.inf)
        top = jnp.max(log_w, axis=1, keepdims=True)
        scores = dots * jnp.exp(log_w - top)
        numer = jnp.dot(scores.astype(BF16), value, preferred_element_type=F32)
        denom = jnp.sum(scores, axis=1, keepdims=True)
        inside.append((cum_t, top, numer, denom))

    for d in range(1, NY):
        j = mod(y + d, NY)
        remote(p1.at[j], p1.at[j], s1.at[0], r1.at[j], y=j).wait_recv()

    def local_piece(j, back):
        ends = p1[j, 64:80].astype(F32)
        if back:
            return joined(ends, 8), joined(ends, 11), p1[j, 32:64].astype(F32), ends[1:2]
        return joined(ends, 2), joined(ends, 5), p1[j, 0:32].astype(F32), ends[0:1]

    for back in (0, 1):
        state, total_decay = empty_state(), jnp.zeros((1, 128), F32)
        for j in reversed(range(NY)) if back else range(NY):
            piece = local_piece(j, back)
            state = step_state(state, piece)
            total_decay = total_decay + piece[1]
        zp[back, 0:32] = state[1].astype(BF16)
        zp[back, 32:48] = jnp.concatenate(
            [state[2], *split3(state[0]), *split3(total_decay), jnp.zeros((9, 128), F32)],
            axis=0,
        ).astype(BF16)
    for d in (8, 7, 9, 6, 10, 5, 11, 4, 12, 3, 13, 2, 14, 1, 15):
        remote(
            zp.at[lax.div(z + d, NZ)],
            p2.at[z],
            s2.at[d - 1],
            r2.at[z],
            z=mod(z + d, NZ),
        ).start()

    mid, end = pl.ds(0, TOK // 2), pl.ds(TOK // 2, TOK // 2)

    def heads_start(i):
        mix, dst = mixes.at[i], full.at[i]
        remote(mix, dst.at[t], hs.at[i], hx.at[i, 0], tp=t_up).start()
        remote(mix, dst.at[t], hs.at[i], hx.at[i, 1], tp=t_down).start()
        remote(mix, dst.at[t], hs.at[i], hc.at[i, 0], tp=partner).start()
        full[i, t] = mixes[i]

    def heads_middle(i):
        mix, dst = mixes.at[i], full.at[i]
        remote(mix, dst.at[t_down], hs.at[i], hx.at[i, 0], tp=t_up).wait_recv()
        src = dst.at[t_down]
        remote(src.at[mid], src.at[mid], hs.at[i], hh.at[i, 0], tp=t_up).start()
        remote(src, src, hs.at[i], hc.at[i, 1], tp=partner).start()
        remote(mix, dst.at[t_up], hs.at[i], hx.at[i, 1], tp=t_up).wait_recv()
        src = dst.at[t_up]
        remote(src.at[end], src.at[end], hs.at[i], hh.at[i, 1], tp=t_down).start()
        remote(src, src, hs.at[i], hc.at[i, 2], tp=partner).start()

    def heads_end(i):
        mix, dst = mixes.at[i], full.at[i]
        for n, part in enumerate((mid, end)):
            src = dst.at[t_far, part]
            remote(src, src, hs.at[i], hh.at[i, n], tp=t_up).wait_recv()
            remote(src, src, hs.at[i], hc.at[i, 3 + n], tp=partner).start()
        remote(mix, dst.at[partner], hs.at[i], hc.at[i, 0], tp=partner).wait_recv()
        remote(mix, dst.at[2 * xd + o], hs.at[i], hc.at[i, 1], tp=partner).wait_recv()
        remote(mix, dst.at[2 * xu + o], hs.at[i], hc.at[i, 2], tp=partner).wait_recv()
        for n, part in enumerate((mid, end)):
            src = dst.at[2 * xo + o, part]
            remote(src, src, hs.at[i], hc.at[i, 3 + n], tp=partner).wait_recv()

    def heads_product(i):
        total = None
        for n in range(NT):
            w = jnp.concatenate(
                [
                    gb[8 * n : 8 * n + 8, at : at + 16].reshape(128, 128)
                    for at in (32 + 32 * i, 48 + 32 * i)
                ],
                axis=1,
            )
            term = jnp.dot(full[i, n], w, preferred_element_type=F32)
            total = term if total is None else total + term
        return total

    to_next.wait_recv()
    to_prev.wait_recv()
    win[0:WINDOW] = halo[0]
    win[WINDOW : WINDOW + TOK] = kv[...]
    win[WINDOW + TOK :] = halo[1]
    low = lax.broadcasted_iota(jnp.int32, (WINDOW, 128), 1) < W_DIM
    two = lax.broadcasted_iota(jnp.int32, (2 * WINDOW, 3 * WINDOW), 0)
    col = lax.broadcasted_iota(jnp.int32, (2 * WINDOW, 3 * WINDOW), 1)
    off = col - jnp.where(two >= WINDOW, two - WINDOW, two)
    in_window = (off >= 0) & (off <= 2 * WINDOW)
    second = lax.broadcasted_iota(jnp.int32, (2 * WINDOW, 1), 0) >= WINDOW
    sink_col = jnp.where(second, sink[0:1, 1:2], sink[0:1, 0:1])
    for b in range(2):
        block = pl.ds(b * WINDOW, WINDOW)
        qb = aq[b * WINDOW : b * WINDOW + WINDOW].astype(F32)
        q0 = jnp.where(low, qb, 0.0)
        q1 = jnp.where(low, pltpu.roll(qb, W_DIM, 1), 0.0)
        qq = jnp.concatenate([q0, q1], axis=0).astype(BF16)
        keys = win[b * WINDOW : b * WINDOW + 3 * WINDOW]
        scores = lax.dot_general(qq, keys, ACROSS, preferred_element_type=F32) * W_DIM**-0.5
        place = me * TOK + (b - 1) * WINDOW + col
        usable = in_window & (place >= 0) & (place < NZ * NY * TOK)
        scores = jnp.where(usable, scores, -jnp.inf)
        peak = jnp.maximum(sink_col, jnp.max(scores, axis=1, keepdims=True))
        weights = jnp.exp(scores - peak)
        tot = jnp.exp(sink_col - peak) + jnp.sum(weights, axis=1, keepdims=True)
        res = jnp.dot(weights.astype(BF16), keys, preferred_element_type=F32) / tot
        mixes[1, block] = jnp.where(
            low, pltpu.roll(res[0:WINDOW], W_DIM, 1), res[WINDOW:]
        ).astype(BF16)
        logt = jnp.transpose(jnp.broadcast_to(peak + jnp.log(tot), (2 * WINDOW, 128)))
        logs[0:1, block] = logt[0:1, 0:WINDOW]
        logs[1:2, block] = logt[0:1, WINDOW:]
    heads_start(1)
    gate_open = 1.0 / (1.0 + jnp.exp(-qkvo[:, 384:512].astype(F32)))
    heads_middle(1)

    for d in range(1, NZ):
        j = mod(z + d, NZ)
        remote(p2.at[j], p2.at[j], s2.at[0], r2.at[j], z=j).wait_recv()

    def far(i, state):
        ends = p2[i, 32:48].astype(F32)
        return step_state(
            state, (joined(ends, 1), joined(ends, 4), p2[i, 0:32].astype(F32), ends[0:1])
        )

    fwd = lax.fori_loop(0, z, far, empty_state())
    bwd = lax.fori_loop(0, NZ - 1 - z, lambda i, s: far(NZ - 1 - i, s), empty_state())
    for j in range(NY):
        p3[j, 0:32] = fwd[1].astype(BF16)
        keep[j, 0:1] = fwd[2]
        keep[j, 2:3] = fwd[0]
        fwd = step_state(fwd, local_piece(j, 0))
    for j in reversed(range(NY)):
        p3[j, 32:64] = bwd[1].astype(BF16)
        keep[j, 1:2] = bwd[2]
        keep[j, 3:4] = bwd[0]
        bwd = step_state(bwd, local_piece(j, 1))
    for d in (2, 1, 3):
        j = mod(y + d, NY)
        remote(p3.at[j], st.at[y], s3.at[d - 1], r3.at[y], y=j).start()
    st[y] = p3[y]
    nm = keep[y]
    heads_end(1)
    acc_b[...] = heads_product(1)
    qf = query.astype(F32) * scale
    for d in range(1, NY):
        j = mod(y + d, NY)
        remote(st.at[j], st.at[j], s3.at[0], r3.at[j], y=j).wait_recv()

    cell = None
    for back in (0, 1):
        cum_t, top_in, numer, denom = inside[back]
        inter = cum_t + nm[2 + back : 3 + back, 0:1]
        top = jnp.maximum(inter, top_in)
        w_in, w_inter = jnp.exp(top_in - top), jnp.exp(inter - top)
        mat = st[:, 32 * back : 32 * back + 32].reshape(128, 128)
        numer = w_in * numer + (w_inter * scale) * jnp.dot(
            query, mat, preferred_element_type=F32
        )
        denom = w_in * denom + w_inter * jnp.sum(
            qf * nm[back : back + 1], axis=1, keepdims=True
        )
        part = numer / jnp.maximum(jnp.abs(denom), jnp.exp(-top))
        cell = part if cell is None else cell + part
    u = cell * gate_open
    norm = lax.rsqrt(jnp.mean(u * u, axis=1, keepdims=True) + EPS)
    mixes[0] = (u * norm * mgain[...]).astype(BF16)
    heads_start(0)
    heads_middle(0)
    heads_end(0)
    out[...] = (acc_b[...] + heads_product(0)).astype(BF16)

    n = NZ * NY - 1
    every = pl.ds(0, n)
    remote(ga.at[every], ga.at[every], sa, az.at[0, 0], y=yd).wait_send()
    remote(gb.at[every], gb.at[every], sb, az.at[0, 0], y=yd).wait_send()
    for d in range(1, NY):
        remote(pk.at[0], p1.at[0], s1.at[d - 1], r1.at[0], y=yd).wait_send()
        remote(p3.at[0], st.at[0], s3.at[d - 1], r3.at[0], y=yd).wait_send()
    for d in range(1, NZ):
        remote(zp.at[0], p2.at[0], s2.at[d - 1], r2.at[0], z=zd).wait_send()
    to_next.wait_send()
    to_prev.wait_send()
    most = pl.ds(0, NT - 1)
    for i in (0, 1):
        src = full.at[i, most]
        remote(src, src, hs.at[i], hc.at[i, 0], tp=partner).wait_send()


def on_device(
    tokens,
    input_norm_gain,
    mq_weight,
    mk_weight,
    mv_weight,
    mo_weight,
    gate_weight,
    gate_bias,
    decay_extra,
    m_gain,
    aq_weight,
    ak_weight,
    av_weight,
    sink_logit,
    out_m_weight,
    out_a_weight,
):
    sds = jax.ShapeDtypeStruct
    dma = pltpu.SemaphoreType.DMA
    vm = pltpu.VMEM
    hbm = pl.BlockSpec(memory_space=pl.ANY)
    local = pl.BlockSpec(memory_space=pltpu.VMEM)
    n = NZ * NY
    return pl.pallas_call(
        layer_body,
        name="layer",
        out_shape=(sds((TOK, 256), BF16), sds((2, TOK), F32)),
        in_specs=[hbm, local, hbm, hbm, hbm, hbm, local, local, local, local]
        + [hbm, local, local, local, hbm, hbm],
        out_specs=[local] * 2,
        scratch_shapes=[
            vm((TOK, D), BF16),
            vm((32, A_COLS), BF16),
            vm((B_ROWS, 128), BF16),
            vm((n, 32, A_COLS), BF16),
            vm((n, B_ROWS, 128), BF16),
            vm((NZ, TOK, 128), BF16),
            vm((TOK, A_COLS), F32),
            vm((TOK, 256), F32),
            vm((TOK, 512), BF16),
            vm((TOK, 128), BF16),
            vm((TOK, 128), BF16),
            vm((2, WINDOW, 128), BF16),
            vm((TOK + 2 * WINDOW, 128), BF16),
            vm((NY, 80, 128), BF16),
            vm((NY, 80, 128), BF16),
            vm((2, 48, 128), BF16),
            vm((NZ, 48, 128), BF16),
            vm((NY, 64, 128), BF16),
            vm((NY, 64, 128), BF16),
            vm((NY, 8, 128), F32),
            vm((2, TOK, 128), BF16),
            vm((2, NT, TOK, 128), BF16),
            dma((10,)),
            dma((2,)),
            dma((2, HALF + 1)),
            dma((2, NZ)),
            dma((2, NZ)),
            dma((2, HALF + 1, NY)),
            dma((2,)),
            dma((2,)),
            dma((NY - 1,)),
            dma((NY,)),
            dma((NZ - 1,)),
            dma((NZ,)),
            dma((NY - 1,)),
            dma((NY,)),
            dma((2,)),
            dma((2,)),
            dma((2,)),
            dma((2, 2)),
            dma((2, 2)),
            dma((2, 5)),
        ],
        compiler_params=pltpu.CompilerParams(collective_id=0, has_side_effects=True),
    )(
        tokens,
        input_norm_gain[None],
        mq_weight,
        mk_weight,
        mv_weight,
        mo_weight,
        gate_weight[:, :, 0].T,
        gate_bias.T,
        decay_extra,
        m_gain[None],
        aq_weight,
        ak_weight,
        av_weight,
        sink_logit[None],
        out_m_weight,
        out_a_weight,
    )


def solution(mesh):
    split = Mesh(mesh.devices.reshape(NZ, NY, NT), ("z", "y", "tp"))
    return jax.shard_map(
        on_device,
        mesh=split,
        in_specs=(
            P(SP, None),
            P(),
            P(SP, "tp"),
            P(SP, "tp"),
            P(SP, "tp"),
            P(SP, "tp"),
            P(SP, None, "tp"),
            P(None, "tp"),
            P(None, "tp", SP),
            P("tp"),
            P(SP, "tp"),
            P(SP, "tp"),
            P(SP, "tp"),
            P("tp"),
            P(SP, "tp"),
            P(SP, "tp"),
        ),
        out_specs=(P(SP, "tp"), P("tp", SP)),
        check_vma=False,
    )
```

time: 113 us -> 85.8 us (0.76)
  Pallas kernels: 106 us -> 82.8 us
  local copies, waits for them, and re-layouts: 4.78 us -> 2.15 us
  other arithmetic: 1.32 us -> 0 us
    pallas_call x6 -> x1, Pallas kernels: 106 us -> 82.8 us  [on_device(): pl.pallas_call(layer_body, name='layer', out_shape=(sds((TOK, 256), BF16)...]
    concatenate x1 -> x0, local copies, waits for them, and re-layouts: 1.5 us -> none  [on_device(): jnp.concatenate([mq_weight, mk_weight, mv_weight, mo_weight, aq_weight, a...]
    concatenate x1 -> x0, other arithmetic: 1.32 us -> none  [on_device(): jnp.concatenate([gate, jnp.concatenate([out_m_weight, out_a_weight], axis...]
    pad x1 -> x0, local copies, waits for them, and re-layouts: 1.25 us -> none  [on_device(): bias = jnp.pad(gate_bias.T, ((0, 0), (0, 124)))]
where the time goes in v2:
time: 85.8 us; the launch traced here: 85.6 us
  Pallas kernels  82.8 us (97%)
  local copies, waits for them, and re-layouts  2.15 us (3%)
    pallas_call x1, Pallas kernels, on_device(): pl.pallas_call(layer_body, name='layer', out_shape=(sds((TOK, 256), BF16)...  82.8 us
    unnamed x4, local copies, waits for them, and re-layouts  2.15 us

profile of v2, /device:TPU:1, one launch (start us, length us, event | category | flops | bytes accessed | tf_op | source)
XLA Modules:
  0.0 85.6 jit_solution(12829100854806385465)
XLA Ops:
  0.6 82.8 %layer.1 = (bf16[256,256]{1,0:T(8,128)(2,1)}, f32[2,256]{1,0:T(2,128)}) custom-call(bf16[256,2048]{1,0:T(8,128)(2,1)} %tok_hbm.1, f32[1,2048]{1,0:T(1,128)} %bitcast.7, bf16[32,128]{1,0:T(8,128)(2,1)} %mq.1, bf16[32,128]{1,0:T(8,128)(2,1)} %mk.1, bf16[32,128]{1,0:T(8,128)(2,1)} %mv.1, bf16[32,128]{1,0:T(8,128)(2,1)} %mo.1, bf16[4,32]{1,0:T(4,128)(2,1)} %bitcast.8, ...), custom_call_target="tpu_custom_call" | custom-call | tf_op jit(solution)/shard_map/layer/pallas_call | solution.py:625
  83.5 0.0 copy-start
  83.5 1.6 %copy.20 = bf16[256,256]{1,0:T(8,128)(2,1)} copy(bf16[256,256]{1,0:T(8,128)(2,1)} %get-tuple-element.4) | data formatting | bytes 262144
  85.1 0.0 copy-done
  85.1 0.6 copy.21
Async XLA Ops:
  83.5 1.6 %copy-start = (f32[2,256]{1,0:T(2,128)S(1)}, f32[2,256]{1,0:T(2,128)}, u32[]{:S(2)}) copy-start(f32[2,256]{1,0:T(2,128)} %get-tuple-element.5) | copy-start | bytes 6148

commit v3 on v2

--- a/solution.py
+++ b/solution.py
@@ -18,7 +18,7 @@
 TOK = 256
 D = 2048
 HALF = NZ // 2
-A_COLS = 640
+A_ROWS = 160
 B_ROWS = 104
 SP = ("z", "y")
 MESH = pl.DeviceIdType.MESH
@@ -107,8 +107,6 @@
     normed,
     acc_a,
     acc_b,
-    qkvo,
-    aq,
     kv,
     halo,
     win,
@@ -163,21 +161,24 @@
         copy = pltpu.make_async_copy(src, dst, local_sem.at[len(loads)])
         copy.start()
         loads.append(copy)
-
-    for i, w in enumerate((mq, mk, mv, mo, aq_w)):
-        load(w, wa.at[:, 128 * i : 128 * i + 128])
+        return copy
+
+    for i, w in enumerate((mk, mv)):
+        load(w, wb.at[32 * i : 32 * i + 32])
+    for i, w in enumerate((mq, mo, aq_w)):
+        load(w, wa.at[32 * i : 32 * i + 32])
     for i, w in enumerate((om, oa)):
         for part in (0, 1):
-            at = 32 + 32 * i + 16 * part
-            load(w.at[:, 128 * part : 128 * part + 128], wb.at[at : at + 16])
-    load(tok_hbm, tok)
+            at = 96 + 32 * i + 16 * part
+            load(w.at[:, 128 * part : 128 * part + 128], wa.at[at : at + 16])
+    tok_load = load(tok_hbm, tok)
     barrier = pltpu.get_barrier_semaphore()
     hello = [{"z": zu}, {"z": zd}, {"y": yu}, {"y": yd}, {"y": yo}]
     hello += [{"z": zn, "y": yn}, {"z": zq, "y": yq}]
     hello += [{"tp": partner}, {"tp": t_up}, {"tp": t_down}]
     for where in hello:
         pl.semaphore_signal(barrier, inc=1, device_id=where, device_id_type=MESH)
-    wb[0:32] = jnp.concatenate([ak_w[...], av_w[...]], axis=1)
+    wb[64:96] = jnp.concatenate([ak_w[...], av_w[...]], axis=1)
     gate_rows = jnp.concatenate([gate_t[...].astype(F32), jnp.zeros((4, 96), F32)], axis=1)
     gate_row = gate_rows[0:1]
     for g in range(1, 4):
@@ -208,24 +209,15 @@
 
     remote(wb, gb.at[me], sb, by.at[0], y=yu).start()
     remote(wb, gb.at[me], sb, by.at[1], y=yd).start()
+    b_up(wb, me, 1, y).start()
+    b_down(wb, me, 1, y).start()
     a_up(wa, me, 1).start()
     a_down(wa, me, 1).start()
-    b_up(wb, me, 1, y).start()
-    b_down(wb, me, 1, y).start()
-    a_side(wa, z)
     ga[me] = wa[...]
     gb[me] = wb[...]
 
-    loads[-1].wait()
-    xs = tok[...].astype(F32)
-    xs = xs * lax.rsqrt(jnp.mean(xs * xs, axis=-1, keepdims=True) + EPS) * gain[...]
-    for i in range(NZ):
-        normed[i] = xs[:, 128 * i : 128 * i + 128].astype(BF16)
-    acc_a[...] = jnp.zeros_like(acc_a)
-    acc_b[...] = jnp.zeros_like(acc_b)
-
     slot_d, slot_u, slot_o = z * NY + yd, z * NY + yu, z * NY + yo
-    lo, hi = pl.ds(0, 16), pl.ds(16, 16)
+    lo, hi = pl.ds(0, A_ROWS // 2), pl.ds(A_ROWS // 2, A_ROWS // 2)
     blo, bhi = pl.ds(0, 48), pl.ds(48, 56)
     remote(wb, gb.at[slot_d], sb, by.at[0], y=yd).wait_recv()
     remote(gb.at[slot_d, blo], gb.at[slot_d, blo], sb, bh.at[0], y=yu).start()
@@ -235,10 +227,22 @@
     remote(gb.at[slot_u, bhi], gb.at[slot_u, bhi], sb, bh.at[1], y=yd).start()
     b_up(gb.at[slot_u], slot_u, 1, yu).start()
     b_down(gb.at[slot_u], slot_u, 1, yu).start()
-    remote(gb.at[slot_o, blo], gb.at[slot_o, blo], sb, bh.at[0], y=yd).wait_recv()
-    remote(gb.at[slot_o, bhi], gb.at[slot_o, bhi], sb, bh.at[1], y=yd).wait_recv()
-    b_up(gb.at[slot_o], slot_o, 1, yo).start()
-    b_down(gb.at[slot_o], slot_o, 1, yo).start()
+    a_side(wa, z)
+
+    def norm():
+        tok_load.wait()
+        xs = tok[...].astype(F32)
+        xs = xs * lax.rsqrt(jnp.mean(xs * xs, axis=-1, keepdims=True) + EPS) * gain[...]
+        for i in range(NZ):
+            normed[i] = xs[:, 128 * i : 128 * i + 128].astype(BF16)
+        acc_a[...] = jnp.zeros_like(acc_a)
+        acc_b[...] = jnp.zeros_like(acc_b)
+
+    def opposite():
+        remote(gb.at[slot_o, blo], gb.at[slot_o, blo], sb, bh.at[0], y=yd).wait_recv()
+        remote(gb.at[slot_o, bhi], gb.at[slot_o, bhi], sb, bh.at[1], y=yd).wait_recv()
+        b_up(gb.at[slot_o], slot_o, 1, yo).start()
+        b_down(gb.at[slot_o], slot_o, 1, yo).start()
 
     def side_forward(zz):
         sd, su = zz * NY + yd, zz * NY + yu
@@ -251,28 +255,33 @@
         lax.broadcasted_iota(jnp.int32, (32, 128), 1), 32
     )
 
-    def level(zz):
+    def stacked(ref, zz, at):
+        return jnp.concatenate([ref[zz * NY + j, at : at + 32] for j in range(NY)], axis=0)
+
+    def level_a(zz):
         so = zz * NY + yo
         remote(ga.at[so, lo], ga.at[so, lo], sa, ah.at[0, zz], y=yd).wait_recv()
         remote(ga.at[so, hi], ga.at[so, hi], sa, ah.at[1, zz], y=yd).wait_recv()
         rows = normed[zz]
-        first = zz * NY
-        for at, width in ((0, 256), (256, 256), (512, 128)):
-            w = jnp.concatenate(
-                [ga[first + j, :, at : at + width] for j in range(NY)], axis=0
-            )
-            acc_a[:, at : at + width] += jnp.dot(rows, w, preferred_element_type=F32)
-        w = jnp.concatenate([gb[first + j, 0:32] for j in range(NY)], axis=0)
+        w = jnp.concatenate([stacked(ga, zz, 0), stacked(ga, zz, 32)], axis=1)
+        acc_a[:, 0:256] += jnp.dot(rows, w, preferred_element_type=F32)
+        acc_a[:, 256:384] += jnp.dot(rows, stacked(ga, zz, 64), preferred_element_type=F32)
+
+    def level_b(zz):
+        rows = normed[zz]
+        w = jnp.concatenate([stacked(gb, zz, 0), stacked(gb, zz, 32)], axis=1)
+        acc_b[:, 0:256] += jnp.dot(rows, w, preferred_element_type=F32)
         g = jnp.concatenate(
             [
-                jnp.where(spread, gb[first + j, 96:104].astype(F32)[0:1], 0.0).astype(BF16)
+                jnp.where(
+                    spread, gb[zz * NY + j, 96:104].astype(F32)[0:1], 0.0
+                ).astype(BF16)
                 for j in range(NY)
             ],
             axis=0,
         )
-        acc_b[...] += jnp.dot(
-            rows, jnp.concatenate([w, g], axis=1), preferred_element_type=F32
-        )
+        w = jnp.concatenate([stacked(gb, zz, 64), g], axis=1)
+        acc_b[:, 256:512] += jnp.dot(rows, w, preferred_element_type=F32)
 
     def both(d, what):
         what(mod(z - d, NZ))
@@ -283,6 +292,28 @@
 
     def step(s, carry):
         z_lo, z_hi = mod(z - s, NZ), mod(z + s, NZ)
+
+        def b_step(j, far_up):
+            sl, sl2 = z_lo * NY + j, z_hi * NY + j
+            up_from, down_from = (HALF, HALF - 1) if far_up else (HALF - 1, HALF)
+
+            @pl.when(s <= up_from)
+            def _():
+                b_up(gb.at[sl], sl, s, j).wait_recv()
+
+                @pl.when(s < up_from)
+                def _():
+                    b_up(gb.at[sl], sl, s + 1, j).start()
+
+            @pl.when(s <= down_from)
+            def _():
+                b_down(gb.at[sl2], sl2, s, j).wait_recv()
+
+                @pl.when(s < down_from)
+                def _():
+                    b_down(gb.at[sl2], sl2, s + 1, j).start()
+
+        b_step(y, True)
         slot = z_lo * NY + y
         a_up(ga.at[slot], slot, s).wait_recv()
 
@@ -303,52 +334,35 @@
 
             a_side(ga.at[slot2], z_hi)
 
-        for j in (y, yd, yu, yo):
-            sl = z_lo * NY + j
-            b_up(gb.at[sl], sl, s, j).wait_recv()
-
-            @pl.when(s < HALF)
-            def _():
-                b_up(gb.at[sl], sl, s + 1, j).start()
-
-            @pl.when(s < HALF)
-            def _():
-                sl2 = z_hi * NY + j
-                b_down(gb.at[sl2], sl2, s, j).wait_recv()
-
-                @pl.when(s < HALF - 1)
-                def _():
-                    b_down(gb.at[sl2], sl2, s + 1, j).start()
+        @pl.when(s == 1)
+        def _():
+            opposite()
+            norm()
+
+        b_step(yd, True)
+        b_step(yu, False)
+        b_step(yo, False)
 
         @pl.when(s >= 2)
         def _():
             both(s - 2, side_forward)
+            both(s - 2, level_b)
 
         @pl.when(s >= 4)
         def _():
-            both(s - 4, level)
+            both(s - 4, level_a)
 
         return carry
 
     lax.fori_loop(1, HALF + 1, step, 0)
-
-    def tail_step(d, carry):
-        @pl.when(d < HALF + 1)
-        def _():
-            both(d, side_forward)
-
-        both(d - 2, level)
-        return carry
-
-    lax.fori_loop(HALF - 1, HALF + 3, tail_step, 0)
-
-    qkvo[...] = acc_a[:, 0:512].astype(BF16)
-    aq[...] = acc_a[:, 512:640].astype(BF16)
-    kv[...] = acc_b[:, 0:128].astype(BF16)
+    both(HALF - 1, level_b)
+    level_b(mod(z - HALF, NZ))
+
+    kv[...] = acc_b[:, 256:384].astype(BF16)
     first, last = pl.ds(0, WINDOW), pl.ds(TOK - WINDOW, WINDOW)
     to_next = remote(kv.at[last], halo.at[0], sh.at[0], rh.at[0], z=zn, y=yn)
     to_prev = remote(kv.at[first], halo.at[1], sh.at[1], rh.at[1], z=zq, y=yq)
-    gt = jnp.sum(jnp.transpose(acc_b[:, 128:256]).reshape(4, 32, TOK), axis=1)
+    gt = jnp.sum(jnp.transpose(acc_b[:, 384:512]).reshape(4, 32, TOK), axis=1)
     in_f, in_b = gt[0:1] + bias[0:1, 0:1], gt[2:3] + bias[0:1, 2:3]
     lf_f = log_sigmoid(gt[1:2] + bias[0:1, 1:2]) + decay[0]
     lf_b = log_sigmoid(gt[3:4] + bias[0:1, 3:4]) + decay[1]
@@ -370,7 +384,7 @@
     w_f, w_b = jnp.exp(end_f - m_f), jnp.exp(end_b - m_b)
     rows = jnp.concatenate([in_f, cum, in_b, rev, w_f, w_b, jnp.zeros((2, TOK), F32)], axis=0)
     cols = jnp.transpose(jnp.concatenate([rows, jnp.zeros((120, TOK), F32)], axis=0))
-    query, key, value = qkvo[:, 0:128], qkvo[:, 128:256], qkvo[:, 256:384]
+    key, value = acc_b[:, 0:128].astype(BF16), acc_b[:, 128:256].astype(BF16)
     val = value.astype(F32)
     tail, mats = [], []
     norms = jnp.dot(rows.astype(BF16), key, preferred_element_type=F32)
@@ -394,21 +408,12 @@
         remote(pk.at[j], p1.at[y], s1.at[d - 1], r1.at[y], y=j).start()
     p1[y] = pk[y]
 
-    scale = M_DIM**-0.5
-    dots = lax.dot_general(query, key, ACROSS, preferred_element_type=F32) * scale
-    ti = lax.broadcasted_iota(jnp.int32, (TOK, TOK), 0)
-    si = lax.broadcasted_iota(jnp.int32, (TOK, TOK), 1)
-    inside = []
-    for back in (0, 1):
-        cum_t = cols[:, 2 * back + 1 : 2 * back + 2]
-        log_in = rows[2 * back : 2 * back + 1] - rows[2 * back + 1 : 2 * back + 2]
-        usable = (si >= ti) if back else (si <= ti)
-        log_w = jnp.where(usable, cum_t + log_in, -jnp.inf)
-        top = jnp.max(log_w, axis=1, keepdims=True)
-        scores = dots * jnp.exp(log_w - top)
-        numer = jnp.dot(scores.astype(BF16), value, preferred_element_type=F32)
-        denom = jnp.sum(scores, axis=1, keepdims=True)
-        inside.append((cum_t, top, numer, denom))
+    both(HALF - 1, side_forward)
+    level_a(mod(z - 5, NZ))
+    level_a(mod(z + 5, NZ))
+    side_forward(mod(z - HALF, NZ))
+    level_a(mod(z - 6, NZ))
+    level_a(mod(z + 6, NZ))
 
     for d in range(1, NY):
         j = mod(y + d, NY)
@@ -427,8 +432,8 @@
             state = step_state(state, piece)
             total_decay = total_decay + piece[1]
         zp[back, 0:32] = state[1].astype(BF16)
-        zp[back, 32:48] = jnp.concatenate(
-            [state[2], *split3(state[0]), *split3(total_decay), jnp.zeros((9, 128), F32)],
+        zp[back, 32:40] = jnp.concatenate(
+            [state[2], *split3(state[0]), *split3(total_decay), jnp.zeros((1, 128), F32)],
             axis=0,
         ).astype(BF16)
     for d in (8, 7, 9, 6, 10, 5, 11, 4, 12, 3, 13, 2, 14, 1, 15):
@@ -439,6 +444,13 @@
             r2.at[z],
             z=mod(z + d, NZ),
         ).start()
+
+    level_a(mod(z - 7, NZ))
+    level_a(mod(z + 7, NZ))
+    level_a(mod(z - HALF, NZ))
+    query = acc_a[:, 0:128].astype(BF16)
+    gate_in = acc_a[:, 128:256].astype(BF16)
+    a_query = acc_a[:, 256:384].astype(BF16).astype(F32)
 
     mid, end = pl.ds(0, TOK // 2), pl.ds(TOK // 2, TOK // 2)
 
@@ -478,8 +490,8 @@
         for n in range(NT):
             w = jnp.concatenate(
                 [
-                    gb[8 * n : 8 * n + 8, at : at + 16].reshape(128, 128)
-                    for at in (32 + 32 * i, 48 + 32 * i)
+                    ga[8 * n : 8 * n + 8, at : at + 16].reshape(128, 128)
+                    for at in (96 + 32 * i, 112 + 32 * i)
                 ],
                 axis=1,
             )
@@ -501,7 +513,7 @@
     sink_col = jnp.where(second, sink[0:1, 1:2], sink[0:1, 0:1])
     for b in range(2):
         block = pl.ds(b * WINDOW, WINDOW)
-        qb = aq[b * WINDOW : b * WINDOW + WINDOW].astype(F32)
+        qb = a_query[b * WINDOW : b * WINDOW + WINDOW]
         q0 = jnp.where(low, qb, 0.0)
         q1 = jnp.where(low, pltpu.roll(qb, W_DIM, 1), 0.0)
         qq = jnp.concatenate([q0, q1], axis=0).astype(BF16)
@@ -521,7 +533,24 @@
         logs[0:1, block] = logt[0:1, 0:WINDOW]
         logs[1:2, block] = logt[0:1, WINDOW:]
     heads_start(1)
-    gate_open = 1.0 / (1.0 + jnp.exp(-qkvo[:, 384:512].astype(F32)))
+    gate_open = 1.0 / (1.0 + jnp.exp(-gate_in.astype(F32)))
+
+    scale = M_DIM**-0.5
+    dots = lax.dot_general(query, key, ACROSS, preferred_element_type=F32) * scale
+    ti = lax.broadcasted_iota(jnp.int32, (TOK, TOK), 0)
+    si = lax.broadcasted_iota(jnp.int32, (TOK, TOK), 1)
+    inside = []
+    for back in (0, 1):
+        cum_t = cols[:, 2 * back + 1 : 2 * back + 2]
+        log_in = rows[2 * back : 2 * back + 1] - rows[2 * back + 1 : 2 * back + 2]
+        usable = (si >= ti) if back else (si <= ti)
+        log_w = jnp.where(usable, cum_t + log_in, -jnp.inf)
+        top = jnp.max(log_w, axis=1, keepdims=True)
+        scores = dots * jnp.exp(log_w - top)
+        numer = jnp.dot(scores.astype(BF16), value, preferred_element_type=F32)
+        denom = jnp.sum(scores, axis=1, keepdims=True)
+        inside.append((cum_t, top, numer, denom))
+
     heads_middle(1)
 
     for d in range(1, NZ):
@@ -529,7 +558,7 @@
         remote(p2.at[j], p2.at[j], s2.at[0], r2.at[j], z=j).wait_recv()
 
     def far(i, state):
-        ends = p2[i, 32:48].astype(F32)
+        ends = p2[i, 32:40].astype(F32)
         return step_state(
             state, (joined(ends, 1), joined(ends, 4), p2[i, 0:32].astype(F32), ends[0:1])
         )
@@ -552,7 +581,7 @@
     st[y] = p3[y]
     nm = keep[y]
     heads_end(1)
-    acc_b[...] = heads_product(1)
+    acc_b[:, 0:256] = heads_product(1)
     qf = query.astype(F32) * scale
     for d in range(1, NY):
         j = mod(y + d, NY)
@@ -579,7 +608,7 @@
     heads_start(0)
     heads_middle(0)
     heads_end(0)
-    out[...] = (acc_b[...] + heads_product(0)).astype(BF16)
+    out[...] = (acc_b[:, 0:256] + heads_product(0)).astype(BF16)
 
     n = NZ * NY - 1
     every = pl.ds(0, n)
@@ -631,22 +660,20 @@
         out_specs=[local] * 2,
         scratch_shapes=[
             vm((TOK, D), BF16),
-            vm((32, A_COLS), BF16),
+            vm((A_ROWS, 128), BF16),
             vm((B_ROWS, 128), BF16),
-            vm((n, 32, A_COLS), BF16),
+            vm((n, A_ROWS, 128), BF16),
             vm((n, B_ROWS, 128), BF16),
             vm((NZ, TOK, 128), BF16),
-            vm((TOK, A_COLS), F32),
-            vm((TOK, 256), F32),
-            vm((TOK, 512), BF16),
-            vm((TOK, 128), BF16),
+            vm((TOK, 384), F32),
+            vm((TOK, 512), F32),
             vm((TOK, 128), BF16),
             vm((2, WINDOW, 128), BF16),
             vm((TOK + 2 * WINDOW, 128), BF16),
             vm((NY, 80, 128), BF16),
             vm((NY, 80, 128), BF16),
-            vm((2, 48, 128), BF16),
-            vm((NZ, 48, 128), BF16),
+            vm((2, 40, 128), BF16),
+            vm((NZ, 40, 128), BF16),
             vm((NY, 64, 128), BF16),
             vm((NY, 64, 128), BF16),
             vm((NY, 8, 128), F32),

time: 85.8 us -> 81 us (0.944)
  Pallas kernels: 82.8 us -> 78 us
    pallas_call x1, Pallas kernels: 82.8 us -> 78 us  [on_device(): pl.pallas_call(layer_body, name='layer', out_shape=(sds((TOK, 256), BF16)...]
where the time goes in v3:
time: 81 us; the launch traced here: 80.8 us
  Pallas kernels  78 us (96%)
  local copies, waits for them, and re-layouts  2.15 us (3%)
    pallas_call x1, Pallas kernels, on_device(): pl.pallas_call(layer_body, name='layer', out_shape=(sds((TOK, 256), BF16)...  78 us
    unnamed x4, local copies, waits for them, and re-layouts  2.15 us

profile of v3, /device:TPU:1, one launch (start us, length us, event | category | flops | bytes accessed | tf_op | source)
XLA Modules:
  0.0 80.8 jit_solution(11439009172871763559)
XLA Ops:
  0.6 78.0 %layer.1 = (bf16[256,256]{1,0:T(8,128)(2,1)}, f32[2,256]{1,0:T(2,128)}) custom-call(bf16[256,2048]{1,0:T(8,128)(2,1)} %tok_hbm.1, f32[1,2048]{1,0:T(1,128)} %bitcast.7, bf16[32,128]{1,0:T(8,128)(2,1)} %mq.1, bf16[32,128]{1,0:T(8,128)(2,1)} %mk.1, bf16[32,128]{1,0:T(8,128)(2,1)} %mv.1, bf16[32,128]{1,0:T(8,128)(2,1)} %mo.1, bf16[4,32]{1,0:T(4,128)(2,1)} %bitcast.8, ...), custom_call_target="tpu_custom_call" | custom-call | tf_op jit(solution)/shard_map/layer/pallas_call | solution.py:654
  78.6 0.0 copy-start
  78.6 1.6 %copy.20 = bf16[256,256]{1,0:T(8,128)(2,1)} copy(bf16[256,256]{1,0:T(8,128)(2,1)} %get-tuple-element.4) | data formatting | bytes 262144
  80.2 0.0 copy-done
  80.2 0.6 copy.21
Async XLA Ops:
  78.6 1.6 %copy-start = (f32[2,256]{1,0:T(2,128)S(1)}, f32[2,256]{1,0:T(2,128)}, u32[]{:S(2)}) copy-start(f32[2,256]{1,0:T(2,128)} %get-tuple-element.5) | copy-start | bytes 6148

commit v4 on v3

--- a/solution.py
+++ b/solution.py
@@ -175,7 +175,7 @@
     barrier = pltpu.get_barrier_semaphore()
     hello = [{"z": zu}, {"z": zd}, {"y": yu}, {"y": yd}, {"y": yo}]
     hello += [{"z": zn, "y": yn}, {"z": zq, "y": yq}]
-    hello += [{"tp": partner}, {"tp": t_up}, {"tp": t_down}]
+    hello += [{"tp": partner}, {"tp": t_up}, {"tp": t_down}, {"tp": t_far}]
     for where in hello:
         pl.semaphore_signal(barrier, inc=1, device_id=where, device_id_type=MESH)
     wb[64:96] = jnp.concatenate([ak_w[...], av_w[...]], axis=1)
@@ -190,11 +190,13 @@
 
     sa, sb = ssem.at[0], ssem.at[1]
 
-    def a_up(src, slot, s):
-        return remote(src, ga.at[slot], sa, az.at[0, s], z=zu)
-
-    def a_down(src, slot, s):
-        return remote(src, ga.at[slot], sa, az.at[1, s], z=zd)
+    parts = (pl.ds(0, A_ROWS // 2), pl.ds(A_ROWS // 2, A_ROWS // 2))
+
+    def a_up(ref, slot, s, h):
+        return remote(ref.at[parts[h]], ga.at[slot, parts[h]], sa, az.at[0, s, h], z=zu)
+
+    def a_down(ref, slot, s, h):
+        return remote(ref.at[parts[h]], ga.at[slot, parts[h]], sa, az.at[1, s, h], z=zd)
 
     def a_side(src, zz):
         slot = zz * NY + y
@@ -211,10 +213,19 @@
     remote(wb, gb.at[me], sb, by.at[1], y=yd).start()
     b_up(wb, me, 1, y).start()
     b_down(wb, me, 1, y).start()
-    a_up(wa, me, 1).start()
-    a_down(wa, me, 1).start()
+    for h in (0, 1):
+        a_up(wa, me, 1, h).start()
+        a_down(wa, me, 1, h).start()
     ga[me] = wa[...]
     gb[me] = wb[...]
+
+    tok_load.wait()
+    xs = tok[...].astype(F32)
+    xs = xs * lax.rsqrt(jnp.mean(xs * xs, axis=-1, keepdims=True) + EPS) * gain[...]
+    for i in range(NZ):
+        normed[i] = xs[:, 128 * i : 128 * i + 128].astype(BF16)
+    acc_a[...] = jnp.zeros_like(acc_a)
+    acc_b[...] = jnp.zeros_like(acc_b)
 
     slot_d, slot_u, slot_o = z * NY + yd, z * NY + yu, z * NY + yo
     lo, hi = pl.ds(0, A_ROWS // 2), pl.ds(A_ROWS // 2, A_ROWS // 2)
@@ -228,15 +239,6 @@
     b_up(gb.at[slot_u], slot_u, 1, yu).start()
     b_down(gb.at[slot_u], slot_u, 1, yu).start()
     a_side(wa, z)
-
-    def norm():
-        tok_load.wait()
-        xs = tok[...].astype(F32)
-        xs = xs * lax.rsqrt(jnp.mean(xs * xs, axis=-1, keepdims=True) + EPS) * gain[...]
-        for i in range(NZ):
-            normed[i] = xs[:, 128 * i : 128 * i + 128].astype(BF16)
-        acc_a[...] = jnp.zeros_like(acc_a)
-        acc_b[...] = jnp.zeros_like(acc_b)
 
     def opposite():
         remote(gb.at[slot_o, blo], gb.at[slot_o, blo], sb, bh.at[0], y=yd).wait_recv()
@@ -290,72 +292,84 @@
         def _():
             what(mod(z + d, NZ))
 
-    def step(s, carry):
+    def b_step(s, j, far_up):
+        sl, sl2 = mod(z - s, NZ) * NY + j, mod(z + s, NZ) * NY + j
+        up_from, down_from = (HALF, HALF - 1) if far_up else (HALF - 1, HALF)
+
+        @pl.when(s <= up_from)
+        def _():
+            b_up(gb.at[sl], sl, s, j).wait_recv()
+
+            @pl.when(s < up_from)
+            def _():
+                b_up(gb.at[sl], sl, s + 1, j).start()
+
+        @pl.when(s <= down_from)
+        def _():
+            b_down(gb.at[sl2], sl2, s, j).wait_recv()
+
+            @pl.when(s < down_from)
+            def _():
+                b_down(gb.at[sl2], sl2, s + 1, j).start()
+
+    def a_step(s):
         z_lo, z_hi = mod(z - s, NZ), mod(z + s, NZ)
-
-        def b_step(j, far_up):
-            sl, sl2 = z_lo * NY + j, z_hi * NY + j
-            up_from, down_from = (HALF, HALF - 1) if far_up else (HALF - 1, HALF)
-
-            @pl.when(s <= up_from)
+        slot, slot2 = z_lo * NY + y, z_hi * NY + y
+        for h in (0, 1):
+            a_up(ga.at[slot], slot, s, h).wait_recv()
+
+            @pl.when(s < HALF)
             def _():
-                b_up(gb.at[sl], sl, s, j).wait_recv()
-
-                @pl.when(s < up_from)
+                a_up(ga.at[slot], slot, s + 1, h).start()
+                a_down(ga.at[slot2], slot2, s, h).wait_recv()
+
+                @pl.when(s < HALF - 1)
                 def _():
-                    b_up(gb.at[sl], sl, s + 1, j).start()
-
-            @pl.when(s <= down_from)
-            def _():
-                b_down(gb.at[sl2], sl2, s, j).wait_recv()
-
-                @pl.when(s < down_from)
-                def _():
-                    b_down(gb.at[sl2], sl2, s + 1, j).start()
-
-        b_step(y, True)
-        slot = z_lo * NY + y
-        a_up(ga.at[slot], slot, s).wait_recv()
+                    a_down(ga.at[slot2], slot2, s + 1, h).start()
+
+        a_side(ga.at[slot], z_lo)
 
         @pl.when(s < HALF)
         def _():
-            a_up(ga.at[slot], slot, s + 1).start()
-
-        a_side(ga.at[slot], z_lo)
-
-        @pl.when(s < HALF)
+            a_side(ga.at[slot2], z_hi)
+
+    def above(d, what):
+        @pl.when(d > 0)
         def _():
-            slot2 = z_hi * NY + y
-            a_down(ga.at[slot2], slot2, s).wait_recv()
-
-            @pl.when(s < HALF - 1)
-            def _():
-                a_down(ga.at[slot2], slot2, s + 1).start()
-
-            a_side(ga.at[slot2], z_hi)
-
-        @pl.when(s == 1)
-        def _():
-            opposite()
-            norm()
-
-        b_step(yd, True)
-        b_step(yu, False)
-        b_step(yo, False)
-
-        @pl.when(s >= 2)
-        def _():
-            both(s - 2, side_forward)
-            both(s - 2, level_b)
+            what(mod(z + d, NZ))
+
+    b_step(1, y, True)
+    opposite()
+    a_step(1)
+    b_step(1, yd, True)
+    b_step(1, yu, False)
+
+    def step(s, carry):
+        b_step(s - 1, yo, False)
+        b_step(s, y, True)
+        level_b(mod(z - s + 2, NZ))
+        a_step(s)
+        above(s - 2, level_b)
+        b_step(s, yd, True)
 
         @pl.when(s >= 4)
         def _():
-            both(s - 4, level_a)
-
+            level_a(mod(z - s + 4, NZ))
+
+        b_step(s, yu, False)
+        both(s - 2, side_forward)
+        above(s - 4, level_a)
         return carry
 
-    lax.fori_loop(1, HALF + 1, step, 0)
+    lax.fori_loop(2, HALF, step, 0)
+    b_step(HALF - 1, yo, False)
+    b_step(HALF, y, True)
+    both(HALF - 2, level_b)
+    b_step(HALF, yd, True)
+    b_step(HALF, yu, False)
+    both(HALF - 2, side_forward)
     both(HALF - 1, level_b)
+    b_step(HALF, yo, False)
     level_b(mod(z - HALF, NZ))
 
     kv[...] = acc_b[:, 256:384].astype(BF16)
@@ -408,12 +422,10 @@
         remote(pk.at[j], p1.at[y], s1.at[d - 1], r1.at[y], y=j).start()
     p1[y] = pk[y]
 
+    a_step(HALF)
+    both(HALF - 4, level_a)
     both(HALF - 1, side_forward)
-    level_a(mod(z - 5, NZ))
-    level_a(mod(z + 5, NZ))
-    side_forward(mod(z - HALF, NZ))
-    level_a(mod(z - 6, NZ))
-    level_a(mod(z + 6, NZ))
+    both(HALF - 3, level_a)
 
     for d in range(1, NY):
         j = mod(y + d, NY)
@@ -445,8 +457,9 @@
             z=mod(z + d, NZ),
         ).start()
 
-    level_a(mod(z - 7, NZ))
-    level_a(mod(z + 7, NZ))
+    side_forward(mod(z - HALF, NZ))
+    both(HALF - 2, level_a)
+    both(HALF - 1, level_a)
     level_a(mod(z - HALF, NZ))
     query = acc_a[:, 0:128].astype(BF16)
     gate_in = acc_a[:, 128:256].astype(BF16)
@@ -456,21 +469,12 @@
 
     def heads_start(i):
         mix, dst = mixes.at[i], full.at[i]
+        for n, part in enumerate((mid, end)):
+            remote(mix.at[part], dst.at[t, part], hs.at[i], hh.at[i, n], tp=t_far).start()
         remote(mix, dst.at[t], hs.at[i], hx.at[i, 0], tp=t_up).start()
         remote(mix, dst.at[t], hs.at[i], hx.at[i, 1], tp=t_down).start()
         remote(mix, dst.at[t], hs.at[i], hc.at[i, 0], tp=partner).start()
         full[i, t] = mixes[i]
-
-    def heads_middle(i):
-        mix, dst = mixes.at[i], full.at[i]
-        remote(mix, dst.at[t_down], hs.at[i], hx.at[i, 0], tp=t_up).wait_recv()
-        src = dst.at[t_down]
-        remote(src.at[mid], src.at[mid], hs.at[i], hh.at[i, 0], tp=t_up).start()
-        remote(src, src, hs.at[i], hc.at[i, 1], tp=partner).start()
-        remote(mix, dst.at[t_up], hs.at[i], hx.at[i, 1], tp=t_up).wait_recv()
-        src = dst.at[t_up]
-        remote(src.at[end], src.at[end], hs.at[i], hh.at[i, 1], tp=t_down).start()
-        remote(src, src, hs.at[i], hc.at[i, 2], tp=partner).start()
 
     def heads_end(i):
         mix, dst = mixes.at[i], full.at[i]
@@ -478,12 +482,16 @@
             src = dst.at[t_far, part]
             remote(src, src, hs.at[i], hh.at[i, n], tp=t_up).wait_recv()
             remote(src, src, hs.at[i], hc.at[i, 3 + n], tp=partner).start()
+        for n, slot in enumerate((t_down, t_up)):
+            src = dst.at[slot]
+            remote(mix, src, hs.at[i], hx.at[i, n], tp=t_up).wait_recv()
+            remote(src, src, hs.at[i], hc.at[i, 1 + n], tp=partner).start()
+        for n, part in enumerate((mid, end)):
+            src = dst.at[2 * xo + o, part]
+            remote(src, src, hs.at[i], hc.at[i, 3 + n], tp=partner).wait_recv()
         remote(mix, dst.at[partner], hs.at[i], hc.at[i, 0], tp=partner).wait_recv()
         remote(mix, dst.at[2 * xd + o], hs.at[i], hc.at[i, 1], tp=partner).wait_recv()
         remote(mix, dst.at[2 * xu + o], hs.at[i], hc.at[i, 2], tp=partner).wait_recv()
-        for n, part in enumerate((mid, end)):
-            src = dst.at[2 * xo + o, part]
-            remote(src, src, hs.at[i], hc.at[i, 3 + n], tp=partner).wait_recv()
 
     def heads_product(i):
         total = None
@@ -551,7 +559,6 @@
         denom = jnp.sum(scores, axis=1, keepdims=True)
         inside.append((cum_t, top, numer, denom))
 
-    heads_middle(1)
 
     for d in range(1, NZ):
         j = mod(z + d, NZ)
@@ -606,14 +613,13 @@
     norm = lax.rsqrt(jnp.mean(u * u, axis=1, keepdims=True) + EPS)
     mixes[0] = (u * norm * mgain[...]).astype(BF16)
     heads_start(0)
-    heads_middle(0)
     heads_end(0)
     out[...] = (acc_b[:, 0:256] + heads_product(0)).astype(BF16)
 
     n = NZ * NY - 1
     every = pl.ds(0, n)
-    remote(ga.at[every], ga.at[every], sa, az.at[0, 0], y=yd).wait_send()
-    remote(gb.at[every], gb.at[every], sb, az.at[0, 0], y=yd).wait_send()
+    remote(ga.at[every], ga.at[every], sa, ah.at[0, 0], y=yd).wait_send()
+    remote(gb.at[every], gb.at[every], sb, ah.at[0, 0], y=yd).wait_send()
     for d in range(1, NY):
         remote(pk.at[0], p1.at[0], s1.at[d - 1], r1.at[0], y=yd).wait_send()
         remote(p3.at[0], st.at[0], s3.at[d - 1], r3.at[0], y=yd).wait_send()
@@ -681,7 +687,7 @@
             vm((2, NT, TOK, 128), BF16),
             dma((10,)),
             dma((2,)),
-            dma((2, HALF + 1)),
+            dma((2, HALF + 1, 2)),
             dma((2, NZ)),
             dma((2, NZ)),
             dma((2, HALF + 1, NY)),

time: 81 us -> 78.4 us (0.968)
  Pallas kernels: 78 us -> 75.4 us
    pallas_call x1, Pallas kernels: 78 us -> 75.4 us  [on_device(): pl.pallas_call(layer_body, name='layer', out_shape=(sds((TOK, 256), BF16)...]
where the time goes in v4:
time: 78.4 us; the launch traced here: 78.2 us
  Pallas kernels  75.4 us (96%)
  local copies, waits for them, and re-layouts  2.15 us (3%)
    pallas_call x1, Pallas kernels, on_device(): pl.pallas_call(layer_body, name='layer', out_shape=(sds((TOK, 256), BF16)...  75.4 us
    unnamed x4, local copies, waits for them, and re-layouts  2.15 us

profile of v4, /device:TPU:1, one launch (start us, length us, event | category | flops | bytes accessed | tf_op | source)
XLA Modules:
  0.0 78.2 jit_solution(16314707410649058470)
XLA Ops:
  0.6 75.4 %layer.1 = (bf16[256,256]{1,0:T(8,128)(2,1)}, f32[2,256]{1,0:T(2,128)}) custom-call(bf16[256,2048]{1,0:T(8,128)(2,1)} %tok_hbm.1, f32[1,2048]{1,0:T(1,128)} %bitcast.7, bf16[32,128]{1,0:T(8,128)(2,1)} %mq.1, bf16[32,128]{1,0:T(8,128)(2,1)} %mk.1, bf16[32,128]{1,0:T(8,128)(2,1)} %mv.1, bf16[32,128]{1,0:T(8,128)(2,1)} %mo.1, bf16[4,32]{1,0:T(4,128)(2,1)} %bitcast.8, ...), custom_call_target="tpu_custom_call" | custom-call | tf_op jit(solution)/shard_map/layer/pallas_call | solution.py:660
  76.0 0.0 copy-start
  76.0 1.6 %copy.20 = bf16[256,256]{1,0:T(8,128)(2,1)} copy(bf16[256,256]{1,0:T(8,128)(2,1)} %get-tuple-element.4) | data formatting | bytes 262144
  77.6 0.0 copy-done
  77.6 0.6 copy.21
Async XLA Ops:
  76.0 1.6 %copy-start = (f32[2,256]{1,0:T(2,128)S(1)}, f32[2,256]{1,0:T(2,128)}, u32[]{:S(2)}) copy-start(f32[2,256]{1,0:T(2,128)} %get-tuple-element.5) | copy-start | bytes 6148

commit v5 on v4

--- a/solution.py
+++ b/solution.py
@@ -82,23 +82,31 @@
 
 def layer_body(
     tok_hbm,
-    gain,
+    gain_hbm,
     mq,
     mk,
     mv,
     mo,
+    gate_hbm,
+    bias_hbm,
+    decay_hbm,
+    mgain_hbm,
+    aq_w,
+    ak_hbm,
+    av_hbm,
+    sink_hbm,
+    om,
+    oa,
+    out,
+    logs,
+    gain,
     gate_t,
     bias,
     decay,
     mgain,
-    aq_w,
     ak_w,
     av_w,
     sink,
-    om,
-    oa,
-    out,
-    logs,
     tok,
     wa,
     wb,
@@ -158,34 +166,40 @@
     loads = []
 
     def load(src, dst):
-        copy = pltpu.make_async_copy(src, dst, local_sem.at[len(loads)])
+        copy = pltpu.make_async_copy(src, dst, local_sem.at[2 + len(loads)])
         copy.start()
         loads.append(copy)
         return copy
 
+    early = [load(ak_hbm, ak_w), load(av_hbm, av_w), load(gate_hbm, gate_t)]
     for i, w in enumerate((mk, mv)):
-        load(w, wb.at[32 * i : 32 * i + 32])
+        pltpu.make_async_copy(w, wb.at[32 * i : 32 * i + 32], local_sem.at[0]).start()
     for i, w in enumerate((mq, mo, aq_w)):
-        load(w, wa.at[32 * i : 32 * i + 32])
+        pltpu.make_async_copy(w, wa.at[32 * i : 32 * i + 32], local_sem.at[1]).start()
     for i, w in enumerate((om, oa)):
         for part in (0, 1):
             at = 96 + 32 * i + 16 * part
-            load(w.at[:, 128 * part : 128 * part + 128], wa.at[at : at + 16])
-    tok_load = load(tok_hbm, tok)
+            src = w.at[:, 128 * part : 128 * part + 128]
+            pltpu.make_async_copy(src, wa.at[at : at + 16], local_sem.at[1]).start()
+    late = [load(tok_hbm, tok), load(gain_hbm, gain), load(bias_hbm, bias)]
+    late += [load(decay_hbm, decay), load(mgain_hbm, mgain), load(sink_hbm, sink)]
     barrier = pltpu.get_barrier_semaphore()
     hello = [{"z": zu}, {"z": zd}, {"y": yu}, {"y": yd}, {"y": yo}]
     hello += [{"z": zn, "y": yn}, {"z": zq, "y": yq}]
     hello += [{"tp": partner}, {"tp": t_up}, {"tp": t_down}, {"tp": t_far}]
     for where in hello:
         pl.semaphore_signal(barrier, inc=1, device_id=where, device_id_type=MESH)
+    for copy in early:
+        copy.wait()
     wb[64:96] = jnp.concatenate([ak_w[...], av_w[...]], axis=1)
     gate_rows = jnp.concatenate([gate_t[...].astype(F32), jnp.zeros((4, 96), F32)], axis=1)
     gate_row = gate_rows[0:1]
     for g in range(1, 4):
         gate_row = gate_row + pltpu.roll(gate_rows[g : g + 1], 32 * g, 1)
     wb[96:104] = jnp.concatenate([gate_row, jnp.zeros((7, 128), F32)], axis=0).astype(BF16)
-    for copy in loads[:-1]:
-        copy.wait()
+    two_weights = wb.at[0:64]
+    pltpu.make_async_copy(two_weights, two_weights, local_sem.at[0]).wait()
+    pltpu.make_async_copy(wa, wa, local_sem.at[1]).wait()
     pl.semaphore_wait(barrier, len(hello))
 
     sa, sb = ssem.at[0], ssem.at[1]
@@ -193,10 +207,10 @@
     parts = (pl.ds(0, A_ROWS // 2), pl.ds(A_ROWS // 2, A_ROWS // 2))
 
     def a_up(ref, slot, s, h):
-        return remote(ref.at[parts[h]], ga.at[slot, parts[h]], sa, az.at[0, s, h], z=zu)
+        return remote(ref.at[parts[h]], ga.at[slot, parts[h]], sa, az.at[0, s - 1, h], z=zu)
 
     def a_down(ref, slot, s, h):
-        return remote(ref.at[parts[h]], ga.at[slot, parts[h]], sa, az.at[1, s, h], z=zd)
+        return remote(ref.at[parts[h]], ga.at[slot, parts[h]], sa, az.at[1, s - 1, h], z=zd)
 
     def a_side(src, zz):
         slot = zz * NY + y
@@ -204,11 +218,12 @@
         remote(src, ga.at[slot], sa, ay.at[1, zz], y=yd).start()
 
     def b_up(src, slot, s, j):
-        return remote(src, gb.at[slot], sb, bz.at[0, s, j], z=zu)
+        return remote(src, gb.at[slot], sb, bz.at[0, s - 1, j], z=zu)
 
     def b_down(src, slot, s, j):
-        return remote(src, gb.at[slot], sb, bz.at[1, s, j], z=zd)
-
+        return remote(src, gb.at[slot], sb, bz.at[1, s - 1, j], z=zd)
+
+    remote(wb, gb.at[me], sb, bh.at[0], y=yo).start()
     remote(wb, gb.at[me], sb, by.at[0], y=yu).start()
     remote(wb, gb.at[me], sb, by.at[1], y=yd).start()
     b_up(wb, me, 1, y).start()
@@ -219,7 +234,8 @@
     ga[me] = wa[...]
     gb[me] = wb[...]
 
-    tok_load.wait()
+    for copy in late:
+        copy.wait()
     xs = tok[...].astype(F32)
     xs = xs * lax.rsqrt(jnp.mean(xs * xs, axis=-1, keepdims=True) + EPS) * gain[...]
     for i in range(NZ):
@@ -229,29 +245,25 @@
 
     slot_d, slot_u, slot_o = z * NY + yd, z * NY + yu, z * NY + yo
     lo, hi = pl.ds(0, A_ROWS // 2), pl.ds(A_ROWS // 2, A_ROWS // 2)
-    blo, bhi = pl.ds(0, 48), pl.ds(48, 56)
     remote(wb, gb.at[slot_d], sb, by.at[0], y=yd).wait_recv()
-    remote(gb.at[slot_d, blo], gb.at[slot_d, blo], sb, bh.at[0], y=yu).start()
     b_up(gb.at[slot_d], slot_d, 1, yd).start()
     b_down(gb.at[slot_d], slot_d, 1, yd).start()
     remote(wb, gb.at[slot_u], sb, by.at[1], y=yd).wait_recv()
-    remote(gb.at[slot_u, bhi], gb.at[slot_u, bhi], sb, bh.at[1], y=yd).start()
     b_up(gb.at[slot_u], slot_u, 1, yu).start()
     b_down(gb.at[slot_u], slot_u, 1, yu).start()
     a_side(wa, z)
 
     def opposite():
-        remote(gb.at[slot_o, blo], gb.at[slot_o, blo], sb, bh.at[0], y=yd).wait_recv()
-        remote(gb.at[slot_o, bhi], gb.at[slot_o, bhi], sb, bh.at[1], y=yd).wait_recv()
+        remote(wb, gb.at[slot_o], sb, bh.at[0], y=yd).wait_recv()
         b_up(gb.at[slot_o], slot_o, 1, yo).start()
         b_down(gb.at[slot_o], slot_o, 1, yo).start()
 
     def side_forward(zz):
         sd, su = zz * NY + yd, zz * NY + yu
         remote(ga.at[sd], ga.at[sd], sa, ay.at[0, zz], y=yd).wait_recv()
-        remote(ga.at[sd, lo], ga.at[sd, lo], sa, ah.at[0, zz], y=yu).start()
+        remote(ga.at[sd, lo], ga.at[sd, lo], sa, ah.at[zz], y=yu).start()
         remote(ga.at[su], ga.at[su], sa, ay.at[1, zz], y=yd).wait_recv()
-        remote(ga.at[su, hi], ga.at[su, hi], sa, ah.at[1, zz], y=yd).start()
+        remote(ga.at[su, hi], ga.at[su, hi], sa, ah.at[zz], y=yd).start()
 
     spread = lax.broadcasted_iota(jnp.int32, (32, 128), 0) == lax.rem(
         lax.broadcasted_iota(jnp.int32, (32, 128), 1), 32
@@ -262,8 +274,7 @@
 
     def level_a(zz):
         so = zz * NY + yo
-        remote(ga.at[so, lo], ga.at[so, lo], sa, ah.at[0, zz], y=yd).wait_recv()
-        remote(ga.at[so, hi], ga.at[so, hi], sa, ah.at[1, zz], y=yd).wait_recv()
+        remote(ga.at[so], ga.at[so], sa, ah.at[zz], y=yd).wait_recv()
         rows = normed[zz]
         w = jnp.concatenate([stacked(ga, zz, 0), stacked(ga, zz, 32)], axis=1)
         acc_a[:, 0:256] += jnp.dot(rows, w, preferred_element_type=F32)
@@ -374,8 +385,8 @@
 
     kv[...] = acc_b[:, 256:384].astype(BF16)
     first, last = pl.ds(0, WINDOW), pl.ds(TOK - WINDOW, WINDOW)
-    to_next = remote(kv.at[last], halo.at[0], sh.at[0], rh.at[0], z=zn, y=yn)
-    to_prev = remote(kv.at[first], halo.at[1], sh.at[1], rh.at[1], z=zq, y=yq)
+    to_next = remote(kv.at[last], halo.at[0], sh, rh, z=zn, y=yn)
+    to_prev = remote(kv.at[first], halo.at[1], sh, rh, z=zq, y=yq)
     gt = jnp.sum(jnp.transpose(acc_b[:, 384:512]).reshape(4, 32, TOK), axis=1)
     in_f, in_b = gt[0:1] + bias[0:1, 0:1], gt[2:3] + bias[0:1, 2:3]
     lf_f = log_sigmoid(gt[1:2] + bias[0:1, 1:2]) + decay[0]
@@ -419,7 +430,7 @@
 
     for d in (2, 1, 3):
         j = mod(y + d, NY)
-        remote(pk.at[j], p1.at[y], s1.at[d - 1], r1.at[y], y=j).start()
+        remote(pk.at[j], p1.at[y], s1, r1, y=j).start()
     p1[y] = pk[y]
 
     a_step(HALF)
@@ -427,9 +438,8 @@
     both(HALF - 1, side_forward)
     both(HALF - 3, level_a)
 
-    for d in range(1, NY):
-        j = mod(y + d, NY)
-        remote(p1.at[j], p1.at[j], s1.at[0], r1.at[j], y=j).wait_recv()
+    others_y, others_z = pl.ds(0, NY - 1), pl.ds(0, NZ - 1)
+    remote(pk.at[others_y], p1.at[others_y], s1, r1, y=yd).wait_recv()
 
     def local_piece(j, back):
         ends = p1[j, 64:80].astype(F32)
@@ -452,8 +462,8 @@
         remote(
             zp.at[lax.div(z + d, NZ)],
             p2.at[z],
-            s2.at[d - 1],
-            r2.at[z],
+            s2,
+            r2,
             z=mod(z + d, NZ),
         ).start()
 
@@ -473,7 +483,7 @@
             remote(mix.at[part], dst.at[t, part], hs.at[i], hh.at[i, n], tp=t_far).start()
         remote(mix, dst.at[t], hs.at[i], hx.at[i, 0], tp=t_up).start()
         remote(mix, dst.at[t], hs.at[i], hx.at[i, 1], tp=t_down).start()
-        remote(mix, dst.at[t], hs.at[i], hc.at[i, 0], tp=partner).start()
+        remote(mix, dst.at[t], hs.at[i], hc.at[i], tp=partner).start()
         full[i, t] = mixes[i]
 
     def heads_end(i):
@@ -481,17 +491,13 @@
         for n, part in enumerate((mid, end)):
             src = dst.at[t_far, part]
             remote(src, src, hs.at[i], hh.at[i, n], tp=t_up).wait_recv()
-            remote(src, src, hs.at[i], hc.at[i, 3 + n], tp=partner).start()
+            remote(src, src, hs.at[i], hc.at[i], tp=partner).start()
         for n, slot in enumerate((t_down, t_up)):
             src = dst.at[slot]
             remote(mix, src, hs.at[i], hx.at[i, n], tp=t_up).wait_recv()
-            remote(src, src, hs.at[i], hc.at[i, 1 + n], tp=partner).start()
-        for n, part in enumerate((mid, end)):
-            src = dst.at[2 * xo + o, part]
-            remote(src, src, hs.at[i], hc.at[i, 3 + n], tp=partner).wait_recv()
-        remote(mix, dst.at[partner], hs.at[i], hc.at[i, 0], tp=partner).wait_recv()
-        remote(mix, dst.at[2 * xd + o], hs.at[i], hc.at[i, 1], tp=partner).wait_recv()
-        remote(mix, dst.at[2 * xu + o], hs.at[i], hc.at[i, 2], tp=partner).wait_recv()
+            remote(src, src, hs.at[i], hc.at[i], tp=partner).start()
+        half = pl.ds(0, NT // 2)
+        remote(dst.at[half], dst.at[half], hs.at[i], hc.at[i], tp=partner).wait_recv()
 
     def heads_product(i):
         total = None
@@ -507,8 +513,7 @@
             total = term if total is None else total + term
         return total
 
-    to_next.wait_recv()
-    to_prev.wait_recv()
+    remote(halo, halo, sh, rh, y=yd).wait_recv()
     win[0:WINDOW] = halo[0]
     win[WINDOW : WINDOW + TOK] = kv[...]
     win[WINDOW + TOK :] = halo[1]
@@ -560,9 +565,7 @@
         inside.append((cum_t, top, numer, denom))
 
 
-    for d in range(1, NZ):
-        j = mod(z + d, NZ)
-        remote(p2.at[j], p2.at[j], s2.at[0], r2.at[j], z=j).wait_recv()
+    remote(p2.at[others_z], p2.at[others_z], s2, r2, z=zd).wait_recv()
 
     def far(i, state):
         ends = p2[i, 32:40].astype(F32)
@@ -584,15 +587,11 @@
         bwd = step_state(bwd, local_piece(j, 1))
     for d in (2, 1, 3):
         j = mod(y + d, NY)
-        remote(p3.at[j], st.at[y], s3.at[d - 1], r3.at[y], y=j).start()
+        remote(p3.at[j], st.at[y], s3, r3, y=j).start()
     st[y] = p3[y]
     nm = keep[y]
-    heads_end(1)
-    acc_b[:, 0:256] = heads_product(1)
     qf = query.astype(F32) * scale
-    for d in range(1, NY):
-        j = mod(y + d, NY)
-        remote(st.at[j], st.at[j], s3.at[0], r3.at[j], y=j).wait_recv()
+    remote(p3.at[others_y], st.at[others_y], s3, r3, y=yd).wait_recv()
 
     cell = None
     for back in (0, 1):
@@ -613,24 +612,23 @@
     norm = lax.rsqrt(jnp.mean(u * u, axis=1, keepdims=True) + EPS)
     mixes[0] = (u * norm * mgain[...]).astype(BF16)
     heads_start(0)
+    heads_end(1)
+    acc_b[:, 0:256] = heads_product(1)
     heads_end(0)
     out[...] = (acc_b[:, 0:256] + heads_product(0)).astype(BF16)
 
     n = NZ * NY - 1
     every = pl.ds(0, n)
-    remote(ga.at[every], ga.at[every], sa, ah.at[0, 0], y=yd).wait_send()
-    remote(gb.at[every], gb.at[every], sb, ah.at[0, 0], y=yd).wait_send()
-    for d in range(1, NY):
-        remote(pk.at[0], p1.at[0], s1.at[d - 1], r1.at[0], y=yd).wait_send()
-        remote(p3.at[0], st.at[0], s3.at[d - 1], r3.at[0], y=yd).wait_send()
-    for d in range(1, NZ):
-        remote(zp.at[0], p2.at[0], s2.at[d - 1], r2.at[0], z=zd).wait_send()
-    to_next.wait_send()
-    to_prev.wait_send()
+    remote(ga.at[every], ga.at[every], sa, ah.at[0], y=yd).wait_send()
+    remote(gb.at[every], gb.at[every], sb, ah.at[0], y=yd).wait_send()
+    remote(pk.at[others_y], p1.at[others_y], s1, r1, y=yd).wait_send()
+    remote(p3.at[others_y], st.at[others_y], s3, r3, y=yd).wait_send()
+    remote(p2.at[others_z], p2.at[others_z], s2, r2, z=zd).wait_send()
+    remote(halo, halo, sh, rh, y=yd).wait_send()
     most = pl.ds(0, NT - 1)
     for i in (0, 1):
         src = full.at[i, most]
-        remote(src, src, hs.at[i], hc.at[i, 0], tp=partner).wait_send()
+        remote(src, src, hs.at[i], hc.at[i], tp=partner).wait_send()
 
 
 def on_device(
@@ -660,11 +658,18 @@
     return pl.pallas_call(
         layer_body,
         name="layer",
-        out_shape=(sds((TOK, 256), BF16), sds((2, TOK), F32)),
-        in_specs=[hbm, local, hbm, hbm, hbm, hbm, local, local, local, local]
-        + [hbm, local, local, local, hbm, hbm],
+        out_shape=(vm((TOK, 256), BF16), vm((2, TOK), F32)),
+        in_specs=[hbm] * 16,
         out_specs=[local] * 2,
         scratch_shapes=[
+            vm((1, D), F32),
+            vm((4, 32), BF16),
+            vm((1, 4), F32),
+            vm((2, 1, TOK), F32),
+            vm((1, 128), F32),
+            vm((32, 64), BF16),
+            vm((32, 64), BF16),
+            vm((1, 2), F32),
             vm((TOK, D), BF16),
             vm((A_ROWS, 128), BF16),
             vm((B_ROWS, 128), BF16),
@@ -685,26 +690,26 @@
             vm((NY, 8, 128), F32),
             vm((2, TOK, 128), BF16),
             vm((2, NT, TOK, 128), BF16),
-            dma((10,)),
+            dma((11,)),
             dma((2,)),
-            dma((2, HALF + 1, 2)),
+            dma((2, HALF, 2)),
             dma((2, NZ)),
-            dma((2, NZ)),
-            dma((2, HALF + 1, NY)),
+            dma((NZ,)),
+            dma((2, HALF, NY)),
             dma((2,)),
             dma((2,)),
-            dma((NY - 1,)),
-            dma((NY,)),
-            dma((NZ - 1,)),
-            dma((NZ,)),
-            dma((NY - 1,)),
-            dma((NY,)),
-            dma((2,)),
-            dma((2,)),
+            dma,
+            dma,
+            dma,
+            dma,
+            dma,
+            dma,
+            dma,
+            dma,
             dma((2,)),
             dma((2, 2)),
             dma((2, 2)),
-            dma((2, 5)),
+            dma((2,)),
         ],
         compiler_params=pltpu.CompilerParams(collective_id=0, has_side_effects=True),
     )(

time: 78.4 us -> 74.3 us (0.948)
  Pallas kernels: 75.4 us -> 72.2 us
  local copies, waits for them, and re-layouts: 2.15 us -> 1.24 us
    pallas_call x1, Pallas kernels: 75.4 us -> 72.2 us  [on_device(): pl.pallas_call(layer_body, name='layer', out_shape=(vm((TOK, 256), BF16),...]
    unnamed x4 -> x2, local copies, waits for them, and re-layouts: 2.15 us -> 1.24 us
where the time goes in v5:
time: 74.3 us; the launch traced here: 74.1 us
  Pallas kernels  72.2 us (97%)
  local copies, waits for them, and re-layouts  1.24 us (2%)
    pallas_call x1, Pallas kernels, on_device(): pl.pallas_call(layer_body, name='layer', out_shape=(vm((TOK, 256), BF16),...  72.2 us

profile of v5, /device:TPU:1, one launch (start us, length us, event | category | flops | bytes accessed | tf_op | source)
XLA Modules:
  0.0 74.1 jit_solution(8258398191505921198)
XLA Ops:
  0.6 72.2 %layer.1 = (bf16[256,256]{1,0:T(8,128)(2,1)S(1)}, f32[2,256]{1,0:T(2,128)S(1)}) custom-call(bf16[256,2048]{1,0:T(8,128)(2,1)} %tok_hbm.1, f32[1,2048]{1,0:T(1,128)} %bitcast.7, bf16[32,128]{1,0:T(8,128)(2,1)} %mq.1, bf16[32,128]{1,0:T(8,128)(2,1)} %mk.1, bf16[32,128]{1,0:T(8,128)(2,1)} %mv.1, bf16[32,128]{1,0:T(8,128)(2,1)} %mo.1, bf16[4,32]{1,0:T(4,128)(2,1)} %bitcast.8, ...), custom_call_target="tpu_custom_call" | custom-call | tf_op jit(solution)/shard_map/layer/pallas_call | solution.py:658
  72.9 0.7 copy.20
  73.5 0.6 copy.21

commit v6 on v5

--- a/solution.py
+++ b/solution.py
@@ -113,6 +113,7 @@
     ga,
     gb,
     normed,
+    tri,
     acc_a,
     acc_b,
     kv,
@@ -207,15 +208,15 @@
     parts = (pl.ds(0, A_ROWS // 2), pl.ds(A_ROWS // 2, A_ROWS // 2))
 
     def a_up(ref, slot, s, h):
-        return remote(ref.at[parts[h]], ga.at[slot, parts[h]], sa, az.at[0, s - 1, h], z=zu)
+        return remote(ref.at[parts[h]], ga.at[slot, parts[h]], sa, az.at[s - 1, h], z=zu)
 
     def a_down(ref, slot, s, h):
-        return remote(ref.at[parts[h]], ga.at[slot, parts[h]], sa, az.at[1, s - 1, h], z=zd)
+        return remote(ref.at[parts[h]], ga.at[slot, parts[h]], sa, az.at[s - 1, h], z=zd)
 
     def a_side(src, zz):
         slot = zz * NY + y
-        remote(src, ga.at[slot], sa, ay.at[0, zz], y=yu).start()
-        remote(src, ga.at[slot], sa, ay.at[1, zz], y=yd).start()
+        remote(src, ga.at[slot], sa, ay.at[zz], y=yu).start()
+        remote(src, ga.at[slot], sa, ay.at[zz], y=yd).start()
 
     def b_up(src, slot, s, j):
         return remote(src, gb.at[slot], sb, bz.at[0, s - 1, j], z=zu)
@@ -242,6 +243,11 @@
         normed[i] = xs[:, 128 * i : 128 * i + 128].astype(BF16)
     acc_a[...] = jnp.zeros_like(acc_a)
     acc_b[...] = jnp.zeros_like(acc_b)
+    down_at = lax.broadcasted_iota(jnp.int32, (TOK, 2 * TOK), 0)
+    across_at = lax.broadcasted_iota(jnp.int32, (TOK, 2 * TOK), 1)
+    upper = (across_at < TOK) & (down_at <= across_at)
+    lower = (across_at >= TOK) & (down_at >= across_at - TOK)
+    tri[...] = jnp.where(upper | lower, 1.0, 0.0).astype(BF16)
 
     slot_d, slot_u, slot_o = z * NY + yd, z * NY + yu, z * NY + yo
     lo, hi = pl.ds(0, A_ROWS // 2), pl.ds(A_ROWS // 2, A_ROWS // 2)
@@ -260,9 +266,9 @@
 
     def side_forward(zz):
         sd, su = zz * NY + yd, zz * NY + yu
-        remote(ga.at[sd], ga.at[sd], sa, ay.at[0, zz], y=yd).wait_recv()
+        two_blocks = ga.at[pl.ds(0, 2)]
+        remote(two_blocks, two_blocks, sa, ay.at[zz], y=yd).wait_recv()
         remote(ga.at[sd, lo], ga.at[sd, lo], sa, ah.at[zz], y=yu).start()
-        remote(ga.at[su], ga.at[su], sa, ay.at[1, zz], y=yd).wait_recv()
         remote(ga.at[su, hi], ga.at[su, hi], sa, ah.at[zz], y=yd).start()
 
     spread = lax.broadcasted_iota(jnp.int32, (32, 128), 0) == lax.rem(
@@ -324,19 +330,24 @@
                 b_down(gb.at[sl2], sl2, s + 1, j).start()
 
     def a_step(s):
+        s = jnp.int32(s)
         z_lo, z_hi = mod(z - s, NZ), mod(z + s, NZ)
         slot, slot2 = z_lo * NY + y, z_hi * NY + y
         for h in (0, 1):
-            a_up(ga.at[slot], slot, s, h).wait_recv()
 
             @pl.when(s < HALF)
             def _():
+                two_halves = ga.at[slot]
+                remote(two_halves, two_halves, sa, az.at[s - 1, h], z=zu).wait_recv()
                 a_up(ga.at[slot], slot, s + 1, h).start()
-                a_down(ga.at[slot2], slot2, s, h).wait_recv()
 
                 @pl.when(s < HALF - 1)
                 def _():
                     a_down(ga.at[slot2], slot2, s + 1, h).start()
+
+            @pl.when(s == HALF)
+            def _():
+                a_up(ga.at[slot], slot, s, h).wait_recv()
 
         a_side(ga.at[slot], z_lo)
 
@@ -394,12 +405,10 @@
     to_next.start()
     to_prev.start()
     lane = lax.broadcasted_iota(jnp.int32, (1, TOK), 1)
-    cum, rev = lf_f, lf_b
-    k = 1
-    while k < TOK:
-        cum = cum + jnp.where(lane >= k, pltpu.roll(cum, k, 1), 0.0)
-        rev = rev + jnp.where(lane < TOK - k, pltpu.roll(rev, TOK - k, 1), 0.0)
-        k *= 2
+    terms = jnp.concatenate([*split3(lf_f), *split3(lf_b), jnp.zeros((2, TOK), F32)], axis=0)
+    sums = jnp.dot(terms.astype(BF16), tri[...], preferred_element_type=F32)
+    cum = joined(sums[:, 0:TOK], 0)
+    rev = joined(sums[:, TOK:], 3)
     tot_f = jnp.max(jnp.where(lane == TOK - 1, cum, -jnp.inf), axis=1, keepdims=True)
     tot_b = jnp.max(jnp.where(lane == 0, rev, -jnp.inf), axis=1, keepdims=True)
     end_f = tot_f - cum + in_f
@@ -676,6 +685,7 @@
             vm((n, A_ROWS, 128), BF16),
             vm((n, B_ROWS, 128), BF16),
             vm((NZ, TOK, 128), BF16),
+            vm((TOK, 2 * TOK), BF16),
             vm((TOK, 384), F32),
             vm((TOK, 512), F32),
             vm((TOK, 128), BF16),
@@ -692,8 +702,8 @@
             vm((2, NT, TOK, 128), BF16),
             dma((11,)),
             dma((2,)),
-            dma((2, HALF, 2)),
-            dma((2, NZ)),
+            dma((HALF, 2)),
+            dma((NZ,)),
             dma((NZ,)),
             dma((2, HALF, NY)),
             dma((2,)),

time: 74.3 us -> 73.5 us (0.989)
  Pallas kernels: 72.2 us -> 71.4 us
    pallas_call x1, Pallas kernels: 72.2 us -> 71.4 us  [on_device(): pl.pallas_call(layer_body, name='layer', out_shape=(vm((TOK, 256), BF16),...]
where the time goes in v6:
time: 73.5 us; the launch traced here: 73.3 us
  Pallas kernels  71.4 us (97%)
  local copies, waits for them, and re-layouts  1.24 us (2%)
    pallas_call x1, Pallas kernels, on_device(): pl.pallas_call(layer_body, name='layer', out_shape=(vm((TOK, 256), BF16),...  71.4 us

profile of v6, /device:TPU:1, one launch (start us, length us, event | category | flops | bytes accessed | tf_op | source)
XLA Modules:
  0.0 73.3 jit_solution(16606501125625689092)
XLA Ops:
  0.6 71.4 %layer.1 = (bf16[256,256]{1,0:T(8,128)(2,1)S(1)}, f32[2,256]{1,0:T(2,128)S(1)}) custom-call(bf16[256,2048]{1,0:T(8,128)(2,1)} %tok_hbm.1, f32[1,2048]{1,0:T(1,128)} %bitcast.7, bf16[32,128]{1,0:T(8,128)(2,1)} %mq.1, bf16[32,128]{1,0:T(8,128)(2,1)} %mk.1, bf16[32,128]{1,0:T(8,128)(2,1)} %mv.1, bf16[32,128]{1,0:T(8,128)(2,1)} %mo.1, bf16[4,32]{1,0:T(4,128)(2,1)} %bitcast.8, ...), custom_call_target="tpu_custom_call" | custom-call | tf_op jit(solution)/shard_map/layer/pallas_call | solution.py:667
  72.1 0.7 copy.20
  72.7 0.6 copy.21

commit v7 on v6

--- a/solution.py
+++ b/solution.py
@@ -164,6 +164,13 @@
     xu, xd, xo = mod(x + 1, NX), mod(x - 1, NX), mod(x + 2, NX)
     partner, t_up, t_down, t_far = 2 * x + o, 2 * xu + c, 2 * xd + c, 2 * xo + c
 
+    barrier = pltpu.get_barrier_semaphore()
+    hello = [{"z": zu}, {"z": zd}, {"y": yu}, {"y": yd}, {"y": yo}]
+    hello += [{"z": zn, "y": yn}, {"z": zq, "y": yq}]
+    hello += [{"tp": partner}, {"tp": t_up}, {"tp": t_down}, {"tp": t_far}]
+    hello += [{"tp": 2 * xu + o}, {"tp": 2 * xd + o}]
+    for where in hello:
+        pl.semaphore_signal(barrier, inc=1, device_id=where, device_id_type=MESH)
     loads = []
 
     def load(src, dst):
@@ -184,12 +191,6 @@
             pltpu.make_async_copy(src, wa.at[at : at + 16], local_sem.at[1]).start()
     late = [load(tok_hbm, tok), load(gain_hbm, gain), load(bias_hbm, bias)]
     late += [load(decay_hbm, decay), load(mgain_hbm, mgain), load(sink_hbm, sink)]
-    barrier = pltpu.get_barrier_semaphore()
-    hello = [{"z": zu}, {"z": zd}, {"y": yu}, {"y": yd}, {"y": yo}]
-    hello += [{"z": zn, "y": yn}, {"z": zq, "y": yq}]
-    hello += [{"tp": partner}, {"tp": t_up}, {"tp": t_down}, {"tp": t_far}]
-    for where in hello:
-        pl.semaphore_signal(barrier, inc=1, device_id=where, device_id_type=MESH)
     for copy in early:
         copy.wait()
     wb[64:96] = jnp.concatenate([ak_w[...], av_w[...]], axis=1)
@@ -229,9 +230,12 @@
     remote(wb, gb.at[me], sb, by.at[1], y=yd).start()
     b_up(wb, me, 1, y).start()
     b_down(wb, me, 1, y).start()
-    for h in (0, 1):
-        a_up(wa, me, 1, h).start()
-        a_down(wa, me, 1, h).start()
+    def a_first():
+        for h in (0, 1):
+            a_up(wa, me, 1, h).start()
+            a_down(wa, me, 1, h).start()
+
+    a_first()
     ga[me] = wa[...]
     gb[me] = wb[...]
 
@@ -492,6 +496,8 @@
             remote(mix.at[part], dst.at[t, part], hs.at[i], hh.at[i, n], tp=t_far).start()
         remote(mix, dst.at[t], hs.at[i], hx.at[i, 0], tp=t_up).start()
         remote(mix, dst.at[t], hs.at[i], hx.at[i, 1], tp=t_down).start()
+        remote(mix, dst.at[t], hs.at[i], hc.at[i], tp=2 * xu + o).start()
+        remote(mix, dst.at[t], hs.at[i], hc.at[i], tp=2 * xd + o).start()
         remote(mix, dst.at[t], hs.at[i], hc.at[i], tp=partner).start()
         full[i, t] = mixes[i]
 
@@ -502,9 +508,7 @@
             remote(src, src, hs.at[i], hh.at[i, n], tp=t_up).wait_recv()
             remote(src, src, hs.at[i], hc.at[i], tp=partner).start()
         for n, slot in enumerate((t_down, t_up)):
-            src = dst.at[slot]
-            remote(mix, src, hs.at[i], hx.at[i, n], tp=t_up).wait_recv()
-            remote(src, src, hs.at[i], hc.at[i], tp=partner).start()
+            remote(mix, dst.at[slot], hs.at[i], hx.at[i, n], tp=t_up).wait_recv()
         half = pl.ds(0, NT // 2)
         remote(dst.at[half], dst.at[half], hs.at[i], hc.at[i], tp=partner).wait_recv()
 

time: 73.5 us -> 73 us (level)
  no operation moved by 1% of the time
where the time goes in v7:
time: 73 us; the launch traced here: 72.8 us
  Pallas kernels  71 us (97%)
  local copies, waits for them, and re-layouts  1.24 us (2%)
    pallas_call x1, Pallas kernels, on_device(): pl.pallas_call(layer_body, name='layer', out_shape=(vm((TOK, 256), BF16),...  71 us

profile of v7, /device:TPU:1, one launch (start us, length us, event | category | flops | bytes accessed | tf_op | source)
XLA Modules:
  0.0 72.8 jit_solution(14942037940108256947)
XLA Ops:
  0.6 71.0 %layer.1 = (bf16[256,256]{1,0:T(8,128)(2,1)S(1)}, f32[2,256]{1,0:T(2,128)S(1)}) custom-call(bf16[256,2048]{1,0:T(8,128)(2,1)} %tok_hbm.1, f32[1,2048]{1,0:T(1,128)} %bitcast.7, bf16[32,128]{1,0:T(8,128)(2,1)} %mq.1, bf16[32,128]{1,0:T(8,128)(2,1)} %mk.1, bf16[32,128]{1,0:T(8,128)(2,1)} %mv.1, bf16[32,128]{1,0:T(8,128)(2,1)} %mo.1, bf16[4,32]{1,0:T(4,128)(2,1)} %bitcast.8, ...), custom_call_target="tpu_custom_call" | custom-call | tf_op jit(solution)/shard_map/layer/pallas_call | solution.py:671
  71.6 0.7 copy.20
  72.3 0.6 copy.21

commit v8 on v7

--- a/solution.py
+++ b/solution.py
@@ -509,15 +509,18 @@
             remote(src, src, hs.at[i], hc.at[i], tp=partner).start()
         for n, slot in enumerate((t_down, t_up)):
             remote(mix, dst.at[slot], hs.at[i], hx.at[i, n], tp=t_up).wait_recv()
+
+    def heads_other(i):
+        dst = full.at[i]
         half = pl.ds(0, NT // 2)
         remote(dst.at[half], dst.at[half], hs.at[i], hc.at[i], tp=partner).wait_recv()
 
-    def heads_product(i):
+    def heads_product(i, slots):
         total = None
-        for n in range(NT):
+        for n in slots:
             w = jnp.concatenate(
                 [
-                    ga[8 * n : 8 * n + 8, at : at + 16].reshape(128, 128)
+                    ga[pl.ds(8 * n, 8), at : at + 16].reshape(128, 128)
                     for at in (96 + 32 * i, 112 + 32 * i)
                 ],
                 axis=1,
@@ -626,9 +629,13 @@
     mixes[0] = (u * norm * mgain[...]).astype(BF16)
     heads_start(0)
     heads_end(1)
-    acc_b[:, 0:256] = heads_product(1)
+    heads_other(1)
+    acc_b[:, 0:256] = heads_product(1, range(NT))
     heads_end(0)
-    out[...] = (acc_b[:, 0:256] + heads_product(0)).astype(BF16)
+    mine = heads_product(0, (t, t_up, t_down, t_far)) + acc_b[:, 0:256]
+    heads_other(0)
+    others = (partner, 2 * xu + o, 2 * xd + o, 2 * xo + o)
+    out[...] = (mine + heads_product(0, others)).astype(BF16)
 
     n = NZ * NY - 1
     every = pl.ds(0, n)

time: 73 us -> 72.7 us (level)
  no operation moved by 1% of the time
where the time goes in v8:
time: 72.7 us; the launch traced here: 72.6 us
  Pallas kernels  70.7 us (97%)
  local copies, waits for them, and re-layouts  1.24 us (2%)
    pallas_call x1, Pallas kernels, on_device(): pl.pallas_call(layer_body, name='layer', out_shape=(vm((TOK, 256), BF16),...  70.7 us

profile of v8, /device:TPU:1, one launch (start us, length us, event | category | flops | bytes accessed | tf_op | source)
XLA Modules:
  0.0 72.6 jit_solution(9920129980780658870)
XLA Ops:
  0.6 70.7 %layer.1 = (bf16[256,256]{1,0:T(8,128)(2,1)S(1)}, f32[2,256]{1,0:T(2,128)S(1)}) custom-call(bf16[256,2048]{1,0:T(8,128)(2,1)} %tok_hbm.1, f32[1,2048]{1,0:T(1,128)} %bitcast.7, bf16[32,128]{1,0:T(8,128)(2,1)} %mq.1, bf16[32,128]{1,0:T(8,128)(2,1)} %mk.1, bf16[32,128]{1,0:T(8,128)(2,1)} %mv.1, bf16[32,128]{1,0:T(8,128)(2,1)} %mo.1, bf16[4,32]{1,0:T(4,128)(2,1)} %bitcast.8, ...), custom_call_target="tpu_custom_call" | custom-call | tf_op jit(solution)/shard_map/layer/pallas_call | solution.py:678
  71.3 0.7 copy.20
  72.0 0.6 copy.21
